TPU v7x, 768 devices: a whole 4x8x12 slice. The times are simulated.
768 devices in a mesh: sp: 96 (over z, y), tp: 8 (over x, core).
Axes of the slice: x: 4, y: 8, z: 12, core: 2. Of those that a mesh axis runs over, the one named last changes fastest.
Arguments:
- prompt_input: bfloat16 [27648, 2048], P('sp'), may hold values from -6 to 6
- next_input: bfloat16 [2048], replicated, may hold values from -6 to 6
- norm_gain: float32 [2048], replicated, may hold values from 0.1 to 1.9
- w_key: bfloat16 [2048, 1024], P(None, 'tp'), may hold values from -0.125 to 0.125
- w_value: bfloat16 [2048, 1024], P(None, 'tp'), may hold values from -0.125 to 0.125
- w_query: bfloat16 [2048, 1024], P(None, 'tp'), may hold values from -0.125 to 0.125
- key_offset: float32 [27648, 8], P('sp', 'tp'), may hold values from -10 to 0, as said below
Outputs:
- key_cache: bfloat16 [96, 96, 3, 1024], P('sp', None, None, 'tp')
- value_cache: bfloat16 [96, 96, 3, 1024], P('sp', None, None, 'tp')
- reading: bfloat16 [1024], replicated
Inputs may be any that keep to these rules, and one draw needn't show every extreme that they name: `key_offset`: finite log-odds offsets, one per key and head.
All inputs are finite; a program needn't handle non-finite values.
Results may differ from a plain program's by a relative error of at most 0.011.
Values may be sent and summed in bfloat16 or wider, within the bound.
No kernel may reach another device: no remote copies, remote signals or barrier semaphores. Data moves between devices by JAX's collectives and lax.ppermute only.
A program may use at most 32 MiB of HBM per device.

v0:
```python
import functools

import jax
import jax.numpy as jnp
from jax import lax
from jax.sharding import Mesh
from jax.sharding import PartitionSpec as P

HEAD_DIM = 128
SP = ("sp_0", "sp_1")
TP = ("tp_0", "tp_1")


def laid_out(tiles, dim):
    tiles = jnp.moveaxis(tiles, 0, dim)
    shape = tiles.shape
    return tiles.reshape(*shape[:dim], shape[dim] * shape[dim + 1], *shape[dim + 2 :])


def all_blocks(shard, axes, order):
    tiles = shard
    for k in order:
        tiles = lax.all_gather(tiles, axes[k])
    done = order[::-1]
    back = [done.index(k) for k in range(len(axes))]
    tiles = tiles.transpose(*back, *range(len(axes), tiles.ndim))
    return tiles.reshape(-1, *shard.shape)


def gathered_by_axis(shard, axes, order, dim):
    return laid_out(all_blocks(shard, axes, order), dim)


def one_axis_at_a_time(shard, axes):
    return functools.reduce(lax.psum, axes, shard)


def whole_of(shard, axes, dim):
    filled = shard
    for number in range(len(axes) - 1, -1, -1):
        filled = lax.all_gather(filled, axes[number], axis=dim, tiled=True)
    return filled


def norm_rows(row_block, gain_vec):
    wide_rows = row_block.astype(jnp.float32)
    inv_rms = lax.rsqrt(jnp.mean(wide_rows * wide_rows, axis=-1, keepdims=True) + 1e-06)
    return (wide_rows * inv_rms * gain_vec).astype(jnp.bfloat16)


def shards(prompt_input, next_input, norm_gain, w_key, w_value, w_query, key_offset):
    span_len = prompt_input.shape[0]
    head_width = w_key.shape[1]
    heads_here = head_width // HEAD_DIM
    score_scale = HEAD_DIM ** (-0.5)
    slots = lax.axis_size(SP)
    sub_len = span_len // slots
    normed = norm_rows(prompt_input, norm_gain)
    key_rows = jnp.dot(normed, w_key, preferred_element_type=jnp.float32).astype(jnp.bfloat16)
    value_rows = jnp.dot(normed, w_value, preferred_element_type=jnp.float32).astype(jnp.bfloat16)
    outgoing = jnp.stack([key_rows, value_rows]).reshape(2, slots, 1, sub_len, head_width)
    arrived = lax.all_to_all(outgoing, SP, split_axis=1, concat_axis=2, tiled=True)
    key_cache = arrived[0]
    value_cache = arrived[1]
    new_query = jnp.dot(
        norm_rows(next_input[None, :], norm_gain), w_query, preferred_element_type=jnp.float32
    )
    new_query = new_query.astype(jnp.bfloat16)
    key_heads = key_rows.reshape(span_len, heads_here, HEAD_DIM)
    value_heads = value_rows.reshape(span_len, heads_here, HEAD_DIM)
    logits = (
        jnp.einsum("hd,shd->sh", new_query, key_heads, preferred_element_type=jnp.float32)
        * score_scale
        + key_offset
    )
    log_breaks = jax.nn.log_sigmoid(-logits)
    inner_sum = lax.cumsum(log_breaks, axis=0, reverse=True) - log_breaks
    block_totals = jnp.sum(log_breaks, axis=0)
    every_total = gathered_by_axis(block_totals[None], SP, (0, 1), 0)
    block_ids = lax.broadcasted_iota(jnp.int32, every_total.shape, 0)
    carried = jnp.sum(jnp.where(block_ids > lax.axis_index(SP), every_total, 0.0), axis=0)
    weights = jnp.exp(jax.nn.log_sigmoid(logits) + inner_sum + carried[None, :])
    partial_value = jnp.einsum("sh,shd->hd", weights, value_heads.astype(jnp.float32))
    summed = one_axis_at_a_time(partial_value, SP)
    own_read = summed.reshape(head_width).astype(jnp.bfloat16)
    reading = whole_of(own_read, TP, 0)
    return (key_cache, value_cache, reading)


def solution(mesh):
    torus = Mesh(mesh.devices.reshape(12, 8, 4, 2), ("sp_0", "sp_1", "tp_0", "tp_1"))
    return jax.shard_map(
        shards,
        mesh=torus,
        in_specs=(P(SP, None), P(), P(), P(None, TP), P(None, TP), P(None, TP), P(SP, TP)),
        out_specs=(P(SP, None, None, TP), P(SP, None, None, TP), P()),
        check_vma=False,
    )
```

profile of v0, /device:TPU:1, one launch (start us, length us, event | category | flops | bytes accessed | tf_op | source)
XLA Modules:
  0.0 127.5 jit_solution(15689701399825729576)
XLA Ops:
  0.6 0.0 copy-start
  0.6 0.0 copy-start.1
  0.7 1.7 %fusion = f32[288]{0:T(512)S(1)} fusion(bf16[288,2048]{1,0:T(8,128)(2,1)} %param.7), kind=kLoop, calls=%fused_computation.2 | loop fusion | flops 1769184 | bytes 1180800 | tf_op jit(solution)/shard_map/reduce_sum | solution.py:47
  2.4 0.0 copy-done
  2.4 0.0 copy-done.1
  2.4 0.0 copy-start.4
  2.4 0.0 copy-start.6
  2.4 1.3 %convolution_convert_fusion = bf16[288,128]{1,0:T(8,128)(2,1)S(1)} fusion(bf16[2048,128]{1,0:T(8,128)(2,1)S(1)} %copy-done, bf16[288,2048]{1,0:T(8,128)(2,1)S(1)} %copy-done.1, f32[2048]{0:T(1024)} %param.9, f32[288]{0:T(512)S(1)} %add_rsqrt_fusion), kind=kOutput, calls=%fused_computation.5 | convolution fusion | flops 153391104 | bytes 1787008 | tf_op jit(solution)/shard_map/dot_general | solution.py:60
  3.7 0.0 copy-done.4
  3.7 0.0 copy-done.6
  3.7 0.5 convolution_convert_fusion.1
  4.3 0.0 copy-start.3
  4.3 0.0 copy-start.2
  4.3 0.0 copy-start.5
  4.4 0.1 pad_maximum_fusion
  4.5 0.9 copy.17
  5.4 22.5 %all-to-all-start = ((bf16[2,96,1,3,128]{4,0,3,2,1:T(2,128)(2,1)}), bf16[2,96,1,3,128]{4,0,3,2,1:T(2,128)(2,1)S(1)}, u32[]{:S(2)}, u32[]{:S(2)}) async-start(bf16[2,96,1,3,128]{4,0,3,2,1:T(2,128)(2,1)} %copy.17), calls=%async_computation | async-start | bytes 294912 | tf_op jit(solution)/shard_map/all_to_all | solution.py:62
  28.0 0.0 copy-done.3
  28.0 0.6 fusion.7
  29.3 0.0 copy-done.2
  29.3 0.3 convolution_reduce_fusion
  29.7 0.0 copy-done.5
  29.7 0.6 fusion.29
  30.9 1.3 %dynamic-slice = u32[1]{0:T(128)} dynamic-slice(u32[768]{0:T(1024)} %constant.38, u32[]{:T(128)S(6)} %add.63), dynamic_slice_sizes={1} | dynamic-slice | bytes 12
  32.2 0.8 dynamic-update-slice
  33.0 1.3 dynamic-slice.1
  34.2 18.5 %all-reduce.1 = f32[12]{0:T(128)S(1)} all-reduce(f32[12]{0:T(128)S(1)} %dynamic-update-slice), channel_id=1, replica_groups=mesh['sp_0'=12,'sp_1'=8,'tp_0'=4,'tp_1'=2] {'sp_0'}, use_global_device_ids=true, to_apply=%add.1 | all-reduce | flops 12 | bytes 96
  53.4 0.2 dynamic-update-slice.1
  53.6 12.8 %all-reduce.2 = f32[96]{0:T(128)S(1)} all-reduce(f32[96]{0:T(128)S(1)} %dynamic-update-slice.1), channel_id=2, replica_groups=mesh['sp_0'=12,'sp_1'=8,'tp_0'=4,'tp_1'=2] {'sp_1'}, use_global_device_ids=true, to_apply=%add.2 | all-reduce | flops 96 | bytes 768
  66.5 1.3 reduce-window.6
  67.7 0.1 slice_reduce_fusion
  67.9 0.2 reduce-window.9
  68.0 0.1 slice_bitcast_fusion
  68.1 0.1 broadcast_bitcast_fusion
  68.2 0.1 reshape.149
  68.3 0.6 fusion.10
  68.9 0.8 fusion.15
  69.7 16.3 %psum.14 = f32[1,128]{1,0:T(1,128)S(1)} all-reduce(f32[1,128]{1,0:T(1,128)S(1)} %fusion.15), channel_id=1, replica_groups=mesh['sp_0'=12,'sp_1'=8,'tp_0'=4,'tp_1'=2] {'sp_0'}, use_global_device_ids=true, to_apply=%region_6.7 | all-reduce | flops 128 | bytes 1024 | tf_op jit(solution)/shard_map/psum | solution.py:35
  86.0 11.7 %psum.15 = bf16[1,128]{1,0:T(2,128)(2,1)S(1)} all-reduce(f32[1,128]{1,0:T(1,128)S(1)} %psum.14), channel_id=1, replica_groups=mesh['sp_0'=12,'sp_1'=8,'tp_0'=4,'tp_1'=2] {'sp_1'}, use_global_device_ids=true, to_apply=%region_7.8 | all-reduce | flops 128 | bytes 768 | tf_op jit(solution)/shard_map/psum | solution.py:35
  97.6 20.6 %all-gather.1 = bf16[1,256]{1,0:T(2,128)(2,1)S(1)} all-gather(bf16[1,128]{1,0:T(2,128)(2,1)S(1)} %psum.15), channel_id=3, replica_groups=mesh['sp_0'=12,'sp_1'=8,'tp_0'=4,'tp_1'=2] {'tp_1'}, dimensions={1}, use_global_device_ids=true | all-gather | bytes 768 | tf_op jit(solution)/shard_map/all_gather | solution.py:41
  118.3 7.7 %all-gather.2 = bf16[1,1024]{1,0:T(2,128)(2,1)S(1)} all-gather(bf16[1,256]{1,0:T(2,128)(2,1)S(1)} %all-gather.1), channel_id=4, replica_groups=mesh['sp_0'=12,'sp_1'=8,'tp_0'=4,'tp_1'=2] {'tp_0'}, dimensions={1}, use_global_device_ids=true | all-gather | bytes 2560 | tf_op jit(solution)/shard_map/all_gather | solution.py:41
  126.0 0.6 reduce.8
  126.6 0.0 all-to-all-done
  126.6 0.2 fusion.30
  126.8 0.7 copy_bitcast_fusion
  (11 shorter events, 0.1 us)
Async XLA Ops:
  0.6 1.7 %copy-start = (bf16[2048,128]{1,0:T(8,128)(2,1)S(1)}, bf16[2048,128]{1,0:T(8,128)(2,1)}, u32[]{:S(2)}) copy-start(bf16[2048,128]{1,0:T(8,128)(2,1)} %param.11) | copy-start | bytes 1572868
  0.6 1.8 %copy-start.1 = (bf16[288,2048]{1,0:T(8,128)(2,1)S(1)}, bf16[288,2048]{1,0:T(8,128)(2,1)}, u32[]{:S(2)}) copy-start(bf16[288,2048]{1,0:T(8,128)(2,1)} %param.7) | copy-start | bytes 3538948
  2.4 1.3 %copy-start.4 = (f32[2048]{0:T(1024)S(1)}, f32[2048]{0:T(1024)}, u32[]{:S(2)}) copy-start(f32[2048]{0:T(1024)} %param.9) | copy-start | bytes 24580
  2.4 1.3 %copy-start.6 = (bf16[2048,128]{1,0:T(8,128)(2,1)S(1)}, bf16[2048,128]{1,0:T(8,128)(2,1)}, u32[]{:S(2)}) copy-start(bf16[2048,128]{1,0:T(8,128)(2,1)} %param.10) | copy-start | bytes 1572868
  4.3 23.7 %copy-start.3 = (bf16[2048]{0:T(1024)(128)(2,1)S(1)}, bf16[2048]{0:T(1024)(128)(2,1)}, u32[]{:S(2)}) copy-start(bf16[2048]{0:T(1024)(128)(2,1)} %param.8) | copy-start | bytes 12292
  4.3 25.0 %copy-start.2 = (bf16[2048,128]{1,0:T(8,128)(2,1)S(1)}, bf16[2048,128]{1,0:T(8,128)(2,1)}, u32[]{:S(2)}) copy-start(bf16[2048,128]{1,0:T(8,128)(2,1)} %param.12) | copy-start | bytes 1572868
  4.3 25.4 %copy-start.5 = (f32[288,1]{0,1:T(1,128)S(1)}, f32[288,1]{0,1:T(1,128)}, u32[]{:S(2)}) copy-start(f32[288,1]{0,1:T(1,128)} %param.13) | copy-start | bytes 3460
  5.4 121.2 %all-to-all-start = ((bf16[2,96,1,3,128]{4,0,3,2,1:T(2,128)(2,1)}), bf16[2,96,1,3,128]{4,0,3,2,1:T(2,128)(2,1)S(1)}, u32[]{:S(2)}, u32[]{:S(2)}) async-start(bf16[2,96,1,3,128]{4,0,3,2,1:T(2,128)(2,1)} %copy.17), calls=%async_computation | async-start | bytes 294912 | tf_op jit(solution)/shard_map/all_to_all | solution.py:62
where the time goes:
time: 128 us; the launch traced here: 127 us
  blocking collectives  87.6 us (68%)
  starting transfers between devices  22.5 us (18%)
  local copies, waits for them, and re-layouts  5.84 us (5%)
  other arithmetic  5.75 us (4%)
  matrix products  2.91 us (2%)
  between operations  2.82 us (2%)
    unnamed x2, blocking collectives  31.3 us
    all_gather x2, blocking collectives, whole_of(): filled = lax.all_gather(filled, axes[number], axis=dim, tiled=True)  28.3 us
    psum x2, blocking collectives, one_axis_at_a_time(): return functools.reduce(lax.psum, axes, shard)  28 us
    all_to_all x1, starting transfers between devices, shards(): lax.all_to_all(outgoing, SP, split_axis=1, concat_axis=2, tiled=True)  22.5 us
    unnamed x21, local copies, waits for them, and re-layouts  3.7 us
  transfers between devices with their start and end apart: 1, of which 0 were waited for; matrix products, arithmetic and copies ran while one was open for 7% of the time, Pallas kernels for 0%

commit v1 on v0

v1 whole, which is shorter than its diff:
```python
import jax
import jax.numpy as jnp
import numpy as np
from jax import lax
from jax.sharding import PartitionSpec as P

HEAD_DIM = 128
SP = "sp"
TP = "tp"
FIRST_RANK = 76


def norm_rows(row_block, gain_vec):
    wide_rows = row_block.astype(jnp.float32)
    inv_rms = lax.rsqrt(jnp.mean(wide_rows * wide_rows, axis=-1, keepdims=True) + 1e-06)
    return (wide_rows * inv_rms * gain_vec).astype(jnp.bfloat16)


def thirds(value):
    high = lax.reduce_precision(value, 8, 7)
    middle = lax.reduce_precision(value - high, 8, 7)
    low = value - high - middle
    return [part.astype(jnp.bfloat16) for part in (high, middle, low)]


def shards(prompt_input, next_input, norm_gain, w_key, w_value, w_query, key_offset):
    span = prompt_input.shape[0]
    slots = lax.axis_size(SP)
    heads = lax.axis_size(TP)
    sub = span // slots
    order = [(r + FIRST_RANK) % slots for r in range(slots)]

    normed = norm_rows(prompt_input, norm_gain)
    keys = jnp.dot(normed, w_key, preferred_element_type=jnp.float32).astype(jnp.bfloat16)
    values = jnp.dot(normed, w_value, preferred_element_type=jnp.float32).astype(jnp.bfloat16)
    query = jnp.dot(norm_rows(next_input[None, :], norm_gain), w_query, preferred_element_type=jnp.float32)
    query = query.astype(jnp.bfloat16)
    logits = lax.dot_general(
        query, keys, (((1,), (1,)), ((), ())), preferred_element_type=jnp.float32
    ) * HEAD_DIM ** (-0.5) + key_offset.reshape(1, span)
    log_breaks = jax.nn.log_sigmoid(-logits)
    inner = lax.cumsum(log_breaks, axis=1, reverse=True) - log_breaks
    total = jnp.sum(log_breaks)
    weights = jnp.exp(jax.nn.log_sigmoid(logits) + inner)
    share = jnp.dot(weights, values.astype(jnp.float32), precision=lax.Precision.HIGHEST)

    turn = lambda rows: jnp.roll(rows.reshape(slots, sub, HEAD_DIM), -FIRST_RANK, axis=0)
    total_row = jnp.concatenate([jnp.stack(thirds(total)), jnp.zeros(HEAD_DIM - 3, jnp.bfloat16)])
    extra = jnp.stack([share[0].astype(jnp.bfloat16), total_row])
    outgoing = jnp.concatenate(
        [turn(keys), turn(values), jnp.broadcast_to(extra[None], (slots, 2, HEAD_DIM))], axis=1
    )
    arrived = lax.all_to_all(
        outgoing, SP, split_axis=0, concat_axis=0, tiled=True, axis_index_groups=[order]
    )
    back = lambda rows: jnp.roll(rows, FIRST_RANK, axis=0)[None]
    key_cache = back(arrived[:, :sub])
    value_cache = back(arrived[:, sub : 2 * sub])

    totals = jnp.sum(arrived[:, 2 * sub + 1, :3].astype(jnp.float32), axis=1)
    place = np.array(order)
    after = jnp.asarray(place[None, :] > place[:, None])
    carried = jnp.sum(jnp.where(after, totals[None, :], 0.0), axis=1)
    shares = arrived[:, 2 * sub].astype(jnp.float32)
    own = jnp.sum(jnp.exp(carried)[:, None] * shares, axis=0).astype(jnp.bfloat16)
    sent = jnp.broadcast_to(own[None, None], (heads, 1, HEAD_DIM))
    reading = lax.all_to_all(sent, TP, split_axis=0, concat_axis=0, tiled=True)
    return key_cache, value_cache, reading.reshape(heads * HEAD_DIM)


def solution(mesh):
    return jax.shard_map(
        shards,
        mesh=mesh,
        in_specs=(P(SP, None), P(), P(), P(None, TP), P(None, TP), P(None, TP), P(SP, TP)),
        out_specs=(P(SP, None, None, TP), P(SP, None, None, TP), P()),
        check_vma=False,
    )
```

time: 128 us -> 58.8 us (0.46)
  blocking collectives: 87.6 us -> 32.6 us
  starting transfers between devices: 22.5 us -> 6.03 us
  waiting for transfers between devices: 0.01 us -> 3.08 us
  between operations: 2.82 us -> 5.88 us
  local copies, waits for them, and re-layouts: 5.84 us -> 2.95 us
  matrix products: 2.91 us -> 1.52 us
    all_to_all x0 -> x1, blocking collectives: none -> 32.6 us  [shards(): lax.all_to_all(outgoing, SP, split_axis=0, concat_axis=0, tiled=True, axi...]
    unnamed x2 -> x0, blocking collectives: 31.3 us -> none
    all_gather x2 -> x0, blocking collectives: 28.3 us -> none  [whole_of(): filled = lax.all_gather(filled, axes[number], axis=dim, tiled=True)]
    psum x2 -> x0, blocking collectives: 28 us -> none  [one_axis_at_a_time(): return functools.reduce(lax.psum, axes, shard)]
    all_to_all x1, starting transfers between devices: 22.5 us -> 6.03 us  [shards(): reading = lax.all_to_all(sent, TP, split_axis=0, concat_axis=0, tiled=True)]
    all_to_all x1, waiting for transfers between devices: 0.01 us -> 3.08 us  [shards(): reading = lax.all_to_all(sent, TP, split_axis=0, concat_axis=0, tiled=True)]
    unnamed x21 -> x19, local copies, waits for them, and re-layouts: 3.7 us -> 1.88 us
  transfers between devices with their start and end apart: 1 -> 1, of which waited for: 0 -> 1; matrix products, arithmetic and copies ran while one was open for 7% -> 3% of each run, Pallas kernels for 0% -> 0%
where the time goes in v1:
time: 58.8 us; the launch traced here: 58.5 us
  blocking collectives  32.6 us (55%)
  other arithmetic  6.45 us (11%)
  starting transfers between devices  6.03 us (10%)
  between operations  5.88 us (10%)
  waiting for transfers between devices  3.08 us (5%)
  local copies, waits for them, and re-layouts  2.95 us (5%)
  matrix products  1.52 us (3%)
    all_to_all x1, blocking collectives, shards(): lax.all_to_all(outgoing, SP, split_axis=0, concat_axis=0, tiled=True, axi...  32.6 us
    all_to_all x1, starting transfers between devices, shards(): reading = lax.all_to_all(sent, TP, split_axis=0, concat_axis=0, tiled=True)  6.03 us
    all_to_all x1, waiting for transfers between devices, shards(): reading = lax.all_to_all(sent, TP, split_axis=0, concat_axis=0, tiled=True)  3.08 us
    reduce_sum x2, other arithmetic, norm_rows(): jnp.mean(wide_rows * wide_rows, axis=-1, keepdims=True) + 1e-06  2.31 us
    unnamed x19, local copies, waits for them, and re-layouts  1.88 us
    another operation x2, other arithmetic  1.44 us
  transfers between devices with their start and end apart: 1, of which 1 were waited for; matrix products, arithmetic and copies ran while one was open for 3% of the time, Pallas kernels for 0%

profile of v1, /device:TPU:1, one launch (start us, length us, event | category | flops | bytes accessed | tf_op | source)
XLA Modules:
  0.0 58.5 jit_solution(4174090627356072562)
XLA Ops:
  0.6 0.0 copy-start
  0.6 0.0 copy-start.1
  0.7 0.0 copy-start.3
  0.7 0.0 copy-start.5
  0.7 1.7 %fusion = f32[288]{0:T(512)S(1)} fusion(bf16[288,2048]{1,0:T(8,128)(2,1)} %param.8), kind=kLoop, calls=%fused_computation.2 | loop fusion | flops 1769184 | bytes 1180800 | tf_op jit(solution)/shard_map/reduce_sum | solution.py:15
  2.4 0.0 copy-done.3
  2.4 0.6 %fusion.10 = f32[]{:T(128)} fusion(bf16[2048]{0:T(1024)(128)(2,1)S(1)} %copy-done.3), kind=kLoop, calls=%fused_computation.24 | loop fusion | flops 6143 | bytes 4100 | tf_op jit(solution)/shard_map/reduce_sum | solution.py:15
  3.7 0.0 copy-done.5
  3.7 0.0 copy-done
  3.7 0.0 copy-done.1
  3.8 0.0 copy-start.6
  3.8 0.0 copy-start.2
  3.8 0.0 copy-start.7
  3.8 0.5 convolution_convert_fusion.1
  4.3 0.1 copy-done.6
  4.5 0.4 copy-done.2
  4.8 0.3 convolution_reduce_fusion
  5.2 0.6 %reduce_sum.56 = f32[]{:T(128)} reduce(f32[288]{0:T(512)S(1)} %get-tuple-element.13, f32[]{:T(128)} %constant.10.clone.1), dimensions={0}, to_apply=%region_4.5 | reduce | flops 287 | bytes 1160 | tf_op jit(solution)/shard_map/reduce_sum | solution.py:43
  10.1 0.0 copy-done.7
  10.1 0.5 convolution_convert_fusion
  10.6 0.0 copy-start.4
  10.7 1.3 %reduce-window.6 = f32[1,3,128]{2,1,0:T(4,128)S(1)} reduce-window(f32[1,3,128]{2,1,0:T(4,128)S(1)} %bitcast.54, f32[]{:T(128)} %constant.10.clone.1), window={size=1x1x128 pad=0_0x0_0x0_127}, to_apply=%region_2.3 | reduce-window | flops 48768 | bytes 3076 | tf_op jit(solution)/shard_map/reduce-window
  12.0 0.1 slice_reduce_fusion
  12.1 0.2 reduce-window.9
  12.3 0.1 slice_bitcast_fusion
  12.3 0.1 broadcast_bitcast_fusion
  12.5 0.2 fusion.4
  12.7 0.1 maximum_bitcast_fusion.2
  12.8 0.2 pad_maximum_fusion
  13.0 32.6 %all_to_all.10 = bf16[96,8,128]{2,1,0:T(8,128)(2,1)S(1)} all-to-all(bf16[96,8,128]{2,1,0:T(8,128)(2,1)S(1)} %pad_maximum_fusion), channel_id=1, replica_groups={{608,616,624,632,640,648,656,664,672,680,688,696,704,712,720,728,736,74..., dimensions={0} | all-to-all | bytes 393216 | tf_op jit(solution)/shard_map/all_to_all | solution.py:53
  45.6 0.8 %fusion.9 = f32[96]{0:T(128)S(1)} fusion(bf16[96,8,128]{2,1,0:T(8,128)(2,1)S(1)} %all_to_all.10), kind=kLoop, calls=%fused_computation.19 | loop fusion | flops 480 | bytes 960 | tf_op jit(solution)/shard_map/reduce_sum | solution.py:60
  46.4 0.0 copy-done.4
  46.4 0.1 select_reduce_fusion
  46.6 0.1 multiply_reduce_fusion
  46.7 0.6 %broadcast_in_dim.46 = bf16[8,1,128]{2,1,0:T(2,128)(2,1)} broadcast(bf16[128]{0:T(256)(128)(2,1)S(1)} %multiply_reduce_fusion), dimensions={2} | broadcast | bytes 2304 | tf_op jit(solution)/shard_map/broadcast_in_dim | solution.py:66
  47.3 6.0 %all-to-all-start.1 = ((bf16[8,1,128]{2,1,0:T(2,128)(2,1)}), bf16[8,1,128]{2,1,0:T(2,128)(2,1)S(1)}, u32[]{:S(2)}, u32[]{:S(2)}) async-start(bf16[8,1,128]{2,1,0:T(2,128)(2,1)} %broadcast_in_dim.46), calls=%async_computation.1 | async-start | bytes 8192 | tf_op jit(solution)/shard_map/all_to_all | solution.py:67
  53.3 0.1 fusion.20
  53.4 0.1 maximum_bitcast_fusion.1
  53.5 0.1 maximum_bitcast_fusion
  53.6 0.6 %copy.20 = bf16[1,96,3,128]{3,1,2,0:T(8,128)(2,1)} copy(bf16[1,96,3,128]{3,2,1,0:T(4,128)(2,1)S(1)} %maximum_bitcast_fusion.1) | data formatting | bytes 147456
  54.2 0.6 %copy.19 = bf16[1,96,3,128]{3,1,2,0:T(8,128)(2,1)} copy(bf16[1,96,3,128]{3,2,1,0:T(4,128)(2,1)S(1)} %maximum_bitcast_fusion) | data formatting | bytes 147456
  54.8 3.1 %all-to-all-done.1 = bf16[8,1,128]{2,1,0:T(2,128)(2,1)S(1)} async-done(((bf16[8,1,128]{2,1,0:T(2,128)(2,1)}), bf16[8,1,128]{2,1,0:T(2,128)(2,1)S(1)}, u32[]{:S(2)}, u32[]{:S(2)}) %all-to-all-start.1) | async-done | bytes 2080 | tf_op jit(solution)/shard_map/all_to_all | solution.py:67
  57.9 0.6 %reduce.9 = bf16[8,128]{1,0:T(8,128)(2,1)} reduce(bf16[8,1,128]{2,1,0:T(2,128)(2,1)S(1)} %all-to-all-done.1, bf16[]{:T(256)} %constant.32), dimensions={1}, to_apply=%all_to_all.7.reduce_sub_computation | reduce | bytes 4098 | tf_op jit(solution)/shard_map/all_to_all | solution.py:67
  (22 shorter events, 0.3 us)
Async XLA Ops:
  0.6 3.1 %copy-start = (bf16[2048,128]{1,0:T(8,128)(2,1)S(1)}, bf16[2048,128]{1,0:T(8,128)(2,1)}, u32[]{:S(2)}) copy-start(bf16[2048,128]{1,0:T(8,128)(2,1)} %param.11) | copy-start | bytes 1572868
  0.6 3.1 %copy-start.1 = (bf16[288,2048]{1,0:T(8,128)(2,1)S(1)}, bf16[288,2048]{1,0:T(8,128)(2,1)}, u32[]{:S(2)}) copy-start(bf16[288,2048]{1,0:T(8,128)(2,1)} %param.8) | copy-start | bytes 3538948
  0.7 1.7 %copy-start.3 = (bf16[2048]{0:T(1024)(128)(2,1)S(1)}, bf16[2048]{0:T(1024)(128)(2,1)}, u32[]{:S(2)}) copy-start(bf16[2048]{0:T(1024)(128)(2,1)} %param.9) | copy-start | bytes 12292
  0.7 3.0 %copy-start.5 = (f32[2048]{0:T(1024)S(1)}, f32[2048]{0:T(1024)}, u32[]{:S(2)}) copy-start(f32[2048]{0:T(1024)} %param.10) | copy-start | bytes 24580
  3.8 0.7 %copy-start.6 = (f32[288,1]{0,1:T(1,128)S(1)}, f32[288,1]{0,1:T(1,128)}, u32[]{:S(2)}) copy-start(f32[288,1]{0,1:T(1,128)} %param.14) | copy-start | bytes 3460
  3.8 1.0 %copy-start.2 = (bf16[2048,128]{1,0:T(8,128)(2,1)S(1)}, bf16[2048,128]{1,0:T(8,128)(2,1)}, u32[]{:S(2)}) copy-start(bf16[2048,128]{1,0:T(8,128)(2,1)} %param.13) | copy-start | bytes 1572868
  3.8 6.3 %copy-start.7 = (bf16[2048,128]{1,0:T(8,128)(2,1)S(1)}, bf16[2048,128]{1,0:T(8,128)(2,1)}, u32[]{:S(2)}) copy-start(bf16[2048,128]{1,0:T(8,128)(2,1)} %param.12) | copy-start | bytes 1572868
  10.6 35.8 %copy-start.4 = (pred[96,96]{1,0:T(32,128)(4,1)S(1)}, pred[96,96]{1,0:T(32,128)(4,1)}, u32[]{:S(2)}) copy-start(pred[96,96]{1,0:T(32,128)(4,1)} %constant.24.clone) | copy-start | bytes 27652
  47.3 10.6 %all-to-all-start.1 = ((bf16[8,1,128]{2,1,0:T(2,128)(2,1)}), bf16[8,1,128]{2,1,0:T(2,128)(2,1)S(1)}, u32[]{:S(2)}, u32[]{:S(2)}) async-start(bf16[8,1,128]{2,1,0:T(2,128)(2,1)} %broadcast_in_dim.46), calls=%async_computation.1 | async-start | bytes 8192 | tf_op jit(solution)/shard_map/all_to_all | solution.py:67

commit v2 on v1

v2 whole, which is shorter than its diff:
```python
import functools

import jax
import jax.numpy as jnp
from jax import lax
from jax.experimental import pallas as pl
from jax.experimental.pallas import tpu as pltpu
from jax.sharding import PartitionSpec as P

HEAD_DIM = 128
LANES = 128
SP = "sp"
TP = "tp"
FIRST_RANK = 76
CHUNK = 96
TP_FIRST = 5


def bf16_parts(value, row, count):
    parts = jnp.zeros_like(value)
    rest = value
    for k in range(count):
        term = rest.astype(jnp.bfloat16).astype(jnp.float32)
        parts = jnp.where(row == k, term, parts)
        rest = rest - term
    return parts.astype(jnp.bfloat16)


def front_kernel(
    x_hbm, next_hbm, gain_hbm, wk_hbm, wv_hbm, wq_hbm, offset_hbm, out_ref,
    x_buf, w_buf, wq_buf, next_buf, gain_buf, offset_buf, normed_buf, k_buf, v_buf, tri_buf, wide_out, sems,
    *, slots, sub,
):
    span, width = x_buf.shape
    chunks = span // CHUNK
    padded = tri_buf.shape[1]
    columns = [pl.ds(c * LANES, LANES) for c in range(width // LANES)]
    copies = {
        "gain": (gain_hbm, gain_buf),
        "x0": (x_hbm.at[pl.ds(0, CHUNK), :], x_buf.at[pl.ds(0, CHUNK), :]),
        "wk": (wk_hbm, w_buf.at[:, pl.ds(0, HEAD_DIM)]),
        "wv": (wv_hbm, w_buf.at[:, pl.ds(HEAD_DIM, HEAD_DIM)]),
        "next": (next_hbm, next_buf),
        "wq": (wq_hbm, wq_buf),
        "offset": (offset_hbm, offset_buf),
    }
    for c in range(1, chunks):
        rows = pl.ds(c * CHUNK, CHUNK)
        copies[f"x{c}"] = (x_hbm.at[rows, :], x_buf.at[rows, :])
    copies = {
        name: pltpu.make_async_copy(source, target, sems.at[number])
        for number, (name, (source, target)) in enumerate(copies.items())
    }
    for copy in copies.values():
        copy.start()

    later = lax.broadcasted_iota(jnp.int32, (span, padded), 0) > lax.broadcasted_iota(jnp.int32, (span, padded), 1)
    beyond = lax.broadcasted_iota(jnp.int32, (span, padded), 1) >= span
    tri_buf[...] = jnp.where(jnp.logical_or(later, beyond), 1.0, 0.0).astype(jnp.bfloat16)

    copies["gain"].wait()
    for c in range(chunks):
        rows = pl.ds(c * CHUNK, CHUNK)
        copies[f"x{c}"].wait()
        squares = jnp.zeros((CHUNK, LANES), jnp.float32)
        for lanes in columns:
            block = x_buf[rows, lanes].astype(jnp.float32)
            squares += block * block
        inv_rms = lax.rsqrt(jnp.sum(squares, axis=1, keepdims=True) * (1.0 / width) + 1e-06)
        for k, lanes in enumerate(columns):
            block = x_buf[rows, lanes].astype(jnp.float32)
            normed_buf[rows, lanes] = (block * inv_rms * gain_buf[k : k + 1, :]).astype(jnp.bfloat16)
        if c == 0:
            copies["wk"].wait()
            copies["wv"].wait()
        both = jnp.dot(normed_buf[rows, :], w_buf[...], preferred_element_type=jnp.float32)
        k_buf[rows, :] = both[:, :HEAD_DIM]
        v_buf[rows, :] = both[:, HEAD_DIM:]

    copies["next"].wait()
    new = next_buf[...].astype(jnp.float32)
    new_inv = lax.rsqrt(jnp.sum(new * new, keepdims=True) * (1.0 / width) + 1e-06)
    new_normed = new * new_inv * gain_buf[...]
    new_row = jnp.concatenate(
        [jnp.broadcast_to(new_normed[k : k + 1, :], (8, LANES)) for k in range(width // LANES)], axis=1
    ).astype(jnp.bfloat16)
    copies["wq"].wait()
    query = jnp.dot(new_row, wq_buf[...], preferred_element_type=jnp.float32).astype(jnp.bfloat16)

    for buf, base in ((k_buf, 0), (v_buf, sub)):
        for k in range(sub):
            for slot, rank, count in (
                (FIRST_RANK, 0, slots - FIRST_RANK),
                (0, slots - FIRST_RANK, FIRST_RANK),
            ):
                wide_out[pl.ds(rank * 8 + base + k, count, stride=8), :] = buf[
                    pl.ds(slot * sub + k, count, stride=sub), :
                ]

    copies["offset"].wait()
    keys = k_buf[...].astype(jnp.bfloat16)
    values = v_buf[...].astype(jnp.bfloat16)
    logits = (
        lax.dot_general(query, keys, (((1,), (1,)), ((), ())), preferred_element_type=jnp.float32)
        * HEAD_DIM ** (-0.5)
        + offset_buf[...]
    )
    row = lax.broadcasted_iota(jnp.int32, (8, span), 0)
    soft = jnp.log1p(jnp.exp(-jnp.abs(logits)))
    log_breaks = -(jnp.maximum(logits, 0.0) + soft)
    log_stops = jnp.minimum(logits, 0.0) - soft
    sums = jnp.sum(
        jnp.dot(bf16_parts(log_breaks, row, 3), tri_buf[...], preferred_element_type=jnp.float32),
        axis=0, keepdims=True,
    )
    weights = jnp.exp(log_stops + sums[:, :span])
    share = jnp.sum(
        jnp.dot(bf16_parts(weights, row, 2), values, preferred_element_type=jnp.float32),
        axis=0, keepdims=True,
    )
    total = sums[:, padded - LANES :]
    lane = lax.broadcasted_iota(jnp.int32, (1, LANES), 1) - (LANES - 3)
    terms = jnp.zeros_like(total)
    rest = total
    for k in range(3):
        term = rest.astype(jnp.bfloat16).astype(jnp.float32)
        terms = jnp.where(lane == k, term, terms)
        rest = rest - term
    wide_out[pl.ds(2 * sub, slots, stride=8), :] = jnp.broadcast_to(share, (slots, LANES))
    wide_out[pl.ds(2 * sub + 1, slots, stride=8), :] = jnp.broadcast_to(terms, (slots, LANES))
    out_ref[...] = wide_out[...].reshape(slots, 8, LANES).astype(jnp.bfloat16)


def front(x, new, gain, w_key, w_value, w_query, offset, slots, sub):
    span, width = x.shape
    padded = -(-(span + 3) // LANES) * LANES
    n_copies = 6 + span // CHUNK
    return pl.pallas_call(
        functools.partial(front_kernel, slots=slots, sub=sub),
        out_shape=pltpu.VMEM((slots, 8, LANES), jnp.bfloat16),
        in_specs=[pl.BlockSpec(memory_space=pl.ANY)] * 7,
        out_specs=pl.BlockSpec(memory_space=pltpu.VMEM),
        scratch_shapes=[
            pltpu.VMEM((span, width), jnp.bfloat16),
            pltpu.VMEM((width, 2 * HEAD_DIM), jnp.bfloat16),
            pltpu.VMEM((width, HEAD_DIM), jnp.bfloat16),
            pltpu.VMEM((width // LANES, LANES), jnp.bfloat16),
            pltpu.VMEM((width // LANES, LANES), jnp.float32),
            pltpu.VMEM((1, span), jnp.float32),
            pltpu.VMEM((span, width), jnp.bfloat16),
            pltpu.VMEM((span, HEAD_DIM), jnp.float32),
            pltpu.VMEM((span, HEAD_DIM), jnp.float32),
            pltpu.VMEM((span, padded), jnp.bfloat16),
            pltpu.VMEM((slots * 8, LANES), jnp.float32),
            pltpu.SemaphoreType.DMA((n_copies,)),
        ],
        name="front",
    )(
        x, new.reshape(width // LANES, LANES), gain.reshape(width // LANES, LANES),
        w_key, w_value, w_query, offset.reshape(1, span),
    )


def join_kernel(arrived_ref, out_ref, wide, *, sub):
    slots = arrived_ref.shape[0]
    wide[...] = arrived_ref[...].astype(jnp.float32).reshape(slots * 8, LANES)
    shares = wide[pl.ds(2 * sub, slots, stride=8), :]
    terms = wide[pl.ds(2 * sub + 1, slots, stride=8), :].astype(jnp.bfloat16)

    def place(dim):
        rank = lax.broadcasted_iota(jnp.int32, (slots, slots), dim)
        return jnp.where(rank < slots - FIRST_RANK, rank + FIRST_RANK, rank + FIRST_RANK - slots)

    after = jnp.where(place(1) > place(0), 1.0, 0.0).astype(jnp.bfloat16)
    carried = jnp.sum(jnp.dot(after, terms, preferred_element_type=jnp.float32), axis=1, keepdims=True)
    own = jnp.sum(jnp.exp(carried) * shares, axis=0, keepdims=True)
    out_ref[...] = jnp.broadcast_to(own[None], out_ref.shape).astype(jnp.bfloat16)


def join(arrived, heads, sub):
    slots = arrived.shape[0]
    return pl.pallas_call(
        functools.partial(join_kernel, sub=sub),
        out_shape=pltpu.VMEM((heads, 1, LANES), jnp.bfloat16),
        in_specs=[pl.BlockSpec(memory_space=pltpu.VMEM)],
        out_specs=pl.BlockSpec(memory_space=pltpu.VMEM),
        scratch_shapes=[pltpu.VMEM((slots * 8, LANES), jnp.float32)],
        name="join",
    )(arrived)


def unpack_kernel(arrived_ref, key_ref, value_ref, wide, cache, *, sub):
    slots = arrived_ref.shape[0]
    wide[...] = arrived_ref[...].astype(jnp.float32).reshape(slots * 8, LANES)
    for out_ref, base in ((key_ref, 0), (value_ref, sub)):
        for k in range(sub):
            for block, rank, count in (
                (FIRST_RANK, 0, slots - FIRST_RANK),
                (0, slots - FIRST_RANK, FIRST_RANK),
            ):
                cache[pl.ds(block, count), :] = wide[pl.ds(rank * 8 + base + k, count, stride=8), :]
            out_ref[k] = cache[...].astype(jnp.bfloat16)


def unpack(arrived, sub):
    slots = arrived.shape[0]
    caches = pl.pallas_call(
        functools.partial(unpack_kernel, sub=sub),
        out_shape=[jax.ShapeDtypeStruct((sub, slots, LANES), jnp.bfloat16)] * 2,
        in_specs=[pl.BlockSpec(memory_space=pltpu.VMEM)],
        out_specs=[pl.BlockSpec(memory_space=pltpu.VMEM)] * 2,
        scratch_shapes=[
            pltpu.VMEM((slots * 8, LANES), jnp.float32),
            pltpu.VMEM((slots, LANES), jnp.float32),
        ],
        name="unpack",
    )(arrived)
    return [cache.transpose(1, 0, 2)[None] for cache in caches]


def finish_kernel(heads_ref, out_ref):
    heads = out_ref.shape[0]
    for r in range(heads):
        h = (r + TP_FIRST) % heads
        out_ref[h : h + 1, :] = heads_ref[r]


def finish(heads_read):
    heads = heads_read.shape[0]
    return pl.pallas_call(
        finish_kernel,
        out_shape=jax.ShapeDtypeStruct((heads, LANES), jnp.bfloat16),
        in_specs=[pl.BlockSpec(memory_space=pltpu.VMEM)],
        out_specs=pl.BlockSpec(memory_space=pltpu.VMEM),
        name="finish",
    )(heads_read).reshape(heads * LANES)


def on_chip(array):
    return pltpu.with_memory_space_constraint(array, pltpu.VMEM)


def shards(prompt_input, next_input, norm_gain, w_key, w_value, w_query, key_offset):
    span = prompt_input.shape[0]
    slots = lax.axis_size(SP)
    heads = lax.axis_size(TP)
    sub = span // slots
    order = [(r + FIRST_RANK) % slots for r in range(slots)]

    outgoing = front(prompt_input, next_input, norm_gain, w_key, w_value, w_query, key_offset, slots, sub)
    arrived = lax.all_to_all(
        outgoing, SP, split_axis=0, concat_axis=0, tiled=True, axis_index_groups=[order]
    )
    arrived = on_chip(arrived)
    own = join( arrived, heads, sub)
    tp_order = [(r + TP_FIRST) % heads for r in range(heads)]
    reading = lax.all_to_all(own, TP, split_axis=0, concat_axis=0, tiled=True, axis_index_groups=[tp_order])
    return *unpack(arrived, sub), finish(on_chip(reading))


def solution(mesh):
    return jax.shard_map(
        shards,
        mesh=mesh,
        in_specs=(P(SP, None), P(), P(), P(None, TP), P(None, TP), P(None, TP), P(SP, TP)),
        out_specs=(P(SP, None, None, TP), P(SP, None, None, TP), P()),
        check_vma=False,
    )
```

time: 58.8 us -> 47.8 us (0.81)
  other arithmetic: 6.45 us -> 0 us
  Pallas kernels: 0 us -> 6.02 us
  between operations: 5.88 us -> 0.64 us
  local copies, waits for them, and re-layouts: 2.95 us -> 0 us
  matrix products: 1.52 us -> 0 us
  waiting for transfers between devices: 3.08 us -> 1.73 us
    pallas_call x0 -> x4, Pallas kernels: none -> 6.02 us  [the longest x1 3.84 us: front(): pl.pallas_call(functools.partial(front_kernel, slots=slots, sub=sub), out...]
    reduce_sum x6 -> x0, other arithmetic: 3.9 us -> none  [the longest x2 2.31 us: norm_rows(): jnp.mean(wide_rows * wide_rows, axis=-1, keepdims=True) + 1e-06]
    unnamed x19 -> x0, local copies, waits for them, and re-layouts: 1.88 us -> none
    another operation x4 -> x0, other arithmetic: 1.53 us -> none
    dot_general x4 -> x0, matrix products: 1.52 us -> none  [the longest x1 0.53 us: shards(): jnp.dot(normed, w_key, preferred_element_type=jnp.float32)]
    all_to_all x1, waiting for transfers between devices: 3.08 us -> 1.73 us  [shards(): lax.all_to_all(own, TP, split_axis=0, concat_axis=0, tiled=True, axis_ind...]
    broadcast_in_dim x3 -> x0, local copies, waits for them, and re-layouts: 0.64 us -> none  [the longest x1 0.6 us: shards(): sent = jnp.broadcast_to(own[None, None], (heads, 1, HEAD_DIM))]
    all_to_all x1 -> x0, other arithmetic: 0.6 us -> none  [shards(): reading = lax.all_to_all(sent, TP, split_axis=0, concat_axis=0, tiled=True)]
  transfers between devices with their start and end apart: 1 -> 1, of which waited for: 1 -> 1; matrix products, arithmetic and copies ran while one was open for 3% -> 0% of each run, Pallas kernels for 0% -> 2%
where the time goes in v2:
time: 47.8 us; the launch traced here: 47.5 us
  blocking collectives  32.6 us (68%)
  starting transfers between devices  6.56 us (14%)
  Pallas kernels  6.02 us (13%)
  waiting for transfers between devices  1.73 us (4%)
  between operations  0.64 us (1%)
    all_to_all x1, blocking collectives, shards(): lax.all_to_all(outgoing, SP, split_axis=0, concat_axis=0, tiled=True, axi...  32.6 us
    all_to_all x1, starting transfers between devices, shards(): lax.all_to_all(own, TP, split_axis=0, concat_axis=0, tiled=True, axis_ind...  6.56 us
    pallas_call x1, Pallas kernels, front(): pl.pallas_call(functools.partial(front_kernel, slots=slots, sub=sub), out...  3.84 us
    all_to_all x1, waiting for transfers between devices, shards(): lax.all_to_all(own, TP, split_axis=0, concat_axis=0, tiled=True, axis_ind...  1.73 us
  transfers between devices with their start and end apart: 1, of which 1 were waited for; matrix products, arithmetic and copies ran while one was open for 0% of the time, Pallas kernels for 2%

profile of v2, /device:TPU:1, one launch (start us, length us, event | category | flops | bytes accessed | tf_op | source)
XLA Modules:
  0.0 47.5 jit_solution(12894666186529852758)
XLA Ops:
  0.6 3.8 %front.1 = bf16[96,8,128]{2,1,0:T(8,128)(2,1)S(1)} custom-call(bf16[288,2048]{1,0:T(8,128)(2,1)} %x_hbm.1, bf16[16,128]{1,0:T(8,128)(2,1)} %bitcast.11, f32[16,128]{1,0:T(8,128)} %bitcast.10, bf16[2048,128]{1,0:T(8,128)(2,1)} %wk_hbm.1, bf16[2048,128]{1,0:T(8,128)(2,1)} %wv_hbm.1, bf16[2048,128]{1,0:T(8,128)(2,1)} %wq_hbm.1, f32[1,288]{1,0:T(1,128)} %bitcast.13), custom_call_target="tpu_custom_call" | custom-call | tf_op jit(solution)/shard_map/front/pallas_call | solution.py:138
  4.5 32.6 %all_to_all.10.arrived_ref = bf16[96,8,128]{2,1,0:T(8,128)(2,1)S(1)} all-to-all(bf16[96,8,128]{2,1,0:T(8,128)(2,1)S(1)} %front.1), channel_id=1, replica_groups={{608,616,624,632,640,648,656,664,672,680,688,696,704,712,720,728,736,74..., dimensions={0} | all-to-all | bytes 393216 | tf_op jit(solution)/shard_map/all_to_all | solution.py:251
  37.1 0.9 %join.1 = bf16[8,1,128]{2,1,0:T(2,128)(2,1)} custom-call(bf16[96,8,128]{2,1,0:T(8,128)(2,1)S(1)} %all_to_all.10.arrived_ref), custom_call_target="tpu_custom_call" | custom-call | tf_op jit(solution)/shard_map/join/pallas_call | solution.py:182
  37.9 6.6 %all-to-all-start.1 = ((bf16[8,1,128]{2,1,0:T(2,128)(2,1)}), bf16[8,1,128]{2,1,0:T(2,128)(2,1)S(1)}, u32[]{:S(2)}, u32[]{:S(2)}) async-start(bf16[8,1,128]{2,1,0:T(2,128)(2,1)} %join.1), calls=%async_computation.1 | async-start | bytes 8192 | tf_op jit(solution)/shard_map/all_to_all | solution.py:257
  44.5 0.7 %unpack.1 = (bf16[3,96,128]{2,1,0:T(8,128)(2,1)}, bf16[3,96,128]{2,1,0:T(8,128)(2,1)}) custom-call(bf16[96,8,128]{2,1,0:T(8,128)(2,1)S(1)} %all_to_all.10.arrived_ref), custom_call_target="tpu_custom_call" | custom-call | tf_op jit(solution)/shard_map/unpack/pallas_call | solution.py:207
  45.2 1.7 %all-to-all-done.1.heads_ref = bf16[8,1,128]{2,1,0:T(2,128)(2,1)S(1)} async-done(((bf16[8,1,128]{2,1,0:T(2,128)(2,1)}), bf16[8,1,128]{2,1,0:T(2,128)(2,1)S(1)}, u32[]{:S(2)}, u32[]{:S(2)}) %all-to-all-start.1) | async-done | bytes 2080 | tf_op jit(solution)/shard_map/all_to_all | solution.py:257
  47.0 0.6 %finish.1 = bf16[8,128]{1,0:T(8,128)(2,1)} custom-call(bf16[8,1,128]{2,1,0:T(2,128)(2,1)S(1)} %all-to-all-done.1.heads_ref), custom_call_target="tpu_custom_call" | custom-call | tf_op jit(solution)/shard_map/finish/pallas_call | solution.py:230
Async XLA Ops:
  37.9 9.0 %all-to-all-start.1 = ((bf16[8,1,128]{2,1,0:T(2,128)(2,1)}), bf16[8,1,128]{2,1,0:T(2,128)(2,1)S(1)}, u32[]{:S(2)}, u32[]{:S(2)}) async-start(bf16[8,1,128]{2,1,0:T(2,128)(2,1)} %join.1), calls=%async_computation.1 | async-start | bytes 8192 | tf_op jit(solution)/shard_map/all_to_all | solution.py:257

commit v3 on v2

--- a/solution.py
+++ b/solution.py
@@ -13,6 +13,7 @@
 TP = "tp"
 FIRST_RANK = 76
 CHUNK = 96
+SLICE = 2048
 TP_FIRST = 5
 
 
@@ -32,36 +33,40 @@
     *, slots, sub,
 ):
     span, width = x_buf.shape
-    chunks = span // CHUNK
     padded = tri_buf.shape[1]
+    row_blocks = [pl.ds(c * CHUNK, CHUNK) for c in range(span // CHUNK)]
+    slices = [pl.ds(c * SLICE, SLICE) for c in range(width // SLICE)]
     columns = [pl.ds(c * LANES, LANES) for c in range(width // LANES)]
-    copies = {
-        "gain": (gain_hbm, gain_buf),
-        "x0": (x_hbm.at[pl.ds(0, CHUNK), :], x_buf.at[pl.ds(0, CHUNK), :]),
-        "wk": (wk_hbm, w_buf.at[:, pl.ds(0, HEAD_DIM)]),
-        "wv": (wv_hbm, w_buf.at[:, pl.ds(HEAD_DIM, HEAD_DIM)]),
-        "next": (next_hbm, next_buf),
-        "wq": (wq_hbm, wq_buf),
-        "offset": (offset_hbm, offset_buf),
-    }
-    for c in range(1, chunks):
-        rows = pl.ds(c * CHUNK, CHUNK)
-        copies[f"x{c}"] = (x_hbm.at[rows, :], x_buf.at[rows, :])
-    copies = {
-        name: pltpu.make_async_copy(source, target, sems.at[number])
-        for number, (name, (source, target)) in enumerate(copies.items())
-    }
-    for copy in copies.values():
+
+    sources = [(gain_hbm, gain_buf), (next_hbm, next_buf), (offset_hbm, offset_buf), (wq_hbm, wq_buf)]
+    sources += [(x_hbm.at[rows, :], x_buf.at[rows, :]) for rows in row_blocks]
+    for rows in slices:
+        sources += [(wk_hbm.at[rows, :], w_buf.at[rows, pl.ds(0, HEAD_DIM)])]
+        sources += [(wv_hbm.at[rows, :], w_buf.at[rows, pl.ds(HEAD_DIM, HEAD_DIM)])]
+    copies = [pltpu.make_async_copy(source, target, sems.at[n]) for n, (source, target) in enumerate(sources)]
+    for copy in copies:
         copy.start()
+    gain_copy, next_copy, offset_copy, wq_copy, *more = copies
+    x_copies, w_copies = more[: len(row_blocks)], more[len(row_blocks) :]
 
     later = lax.broadcasted_iota(jnp.int32, (span, padded), 0) > lax.broadcasted_iota(jnp.int32, (span, padded), 1)
     beyond = lax.broadcasted_iota(jnp.int32, (span, padded), 1) >= span
     tri_buf[...] = jnp.where(jnp.logical_or(later, beyond), 1.0, 0.0).astype(jnp.bfloat16)
 
-    copies["gain"].wait()
-    for c in range(chunks):
-        rows = pl.ds(c * CHUNK, CHUNK)
-        copies[f"x{c}"].wait()
+    gain_copy.wait()
+    next_copy.wait()
+    new = next_buf[...].astype(jnp.float32)
+    new_inv = lax.rsqrt(jnp.sum(new * new, keepdims=True) * (1.0 / width) + 1e-06)
+    new_normed = new * new_inv * gain_buf[...]
+    new_row = jnp.concatenate(
+        [jnp.broadcast_to(new_normed[k : k + 1, :], (8, LANES)) for k in range(width // LANES)], axis=1
+    ).astype(jnp.bfloat16)
+    offset_copy.wait()
+    wq_copy.wait()
+    query = jnp.dot(new_row, wq_buf[...], preferred_element_type=jnp.float32).astype(jnp.bfloat16)
+
+    for rows, copy in zip(row_blocks, x_copies):
+        copy.wait()
         squares = jnp.zeros((CHUNK, LANES), jnp.float32)
         for lanes in columns:
             block = x_buf[rows, lanes].astype(jnp.float32)
@@ -70,22 +75,35 @@
         for k, lanes in enumerate(columns):
             block = x_buf[rows, lanes].astype(jnp.float32)
             normed_buf[rows, lanes] = (block * inv_rms * gain_buf[k : k + 1, :]).astype(jnp.bfloat16)
-        if c == 0:
-            copies["wk"].wait()
-            copies["wv"].wait()
-        both = jnp.dot(normed_buf[rows, :], w_buf[...], preferred_element_type=jnp.float32)
-        k_buf[rows, :] = both[:, :HEAD_DIM]
-        v_buf[rows, :] = both[:, HEAD_DIM:]
-
-    copies["next"].wait()
-    new = next_buf[...].astype(jnp.float32)
-    new_inv = lax.rsqrt(jnp.sum(new * new, keepdims=True) * (1.0 / width) + 1e-06)
-    new_normed = new * new_inv * gain_buf[...]
-    new_row = jnp.concatenate(
-        [jnp.broadcast_to(new_normed[k : k + 1, :], (8, LANES)) for k in range(width // LANES)], axis=1
-    ).astype(jnp.bfloat16)
-    copies["wq"].wait()
-    query = jnp.dot(new_row, wq_buf[...], preferred_element_type=jnp.float32).astype(jnp.bfloat16)
+
+    w_copies[0].wait()
+    w_copies[1].wait()
+    both = jnp.concatenate([
+        jnp.dot(normed_buf[r : r + 144, :], w_buf[...], preferred_element_type=jnp.float32)
+        for r in range(0, span, 144)
+    ], axis=0)
+    k_buf[...] = both[:, :HEAD_DIM]
+    v_buf[...] = both[:, HEAD_DIM:]
+    keys = both[:, :HEAD_DIM].astype(jnp.bfloat16)
+    values = both[:, HEAD_DIM:].astype(jnp.bfloat16)
+    logits = (
+        lax.dot_general(query, keys, (((1,), (1,)), ((), ())), preferred_element_type=jnp.float32)
+        * HEAD_DIM ** (-0.5)
+        + offset_buf[...]
+    )
+    row = lax.broadcasted_iota(jnp.int32, (8, span), 0)
+    soft = jnp.log1p(jnp.exp(-jnp.abs(logits)))
+    log_breaks = -(jnp.maximum(logits, 0.0) + soft)
+    log_stops = jnp.minimum(logits, 0.0) - soft
+    sums = jnp.sum(
+        jnp.dot(bf16_parts(log_breaks, row, 3), tri_buf[...], preferred_element_type=jnp.float32),
+        axis=0, keepdims=True,
+    )
+    weights = jnp.exp(log_stops + sums[:, :span])
+    share = jnp.sum(
+        jnp.dot(bf16_parts(weights, row, 2), values, preferred_element_type=jnp.float32),
+        axis=0, keepdims=True,
+    )
 
     for buf, base in ((k_buf, 0), (v_buf, sub)):
         for k in range(sub):
@@ -97,27 +115,6 @@
                     pl.ds(slot * sub + k, count, stride=sub), :
                 ]
 
-    copies["offset"].wait()
-    keys = k_buf[...].astype(jnp.bfloat16)
-    values = v_buf[...].astype(jnp.bfloat16)
-    logits = (
-        lax.dot_general(query, keys, (((1,), (1,)), ((), ())), preferred_element_type=jnp.float32)
-        * HEAD_DIM ** (-0.5)
-        + offset_buf[...]
-    )
-    row = lax.broadcasted_iota(jnp.int32, (8, span), 0)
-    soft = jnp.log1p(jnp.exp(-jnp.abs(logits)))
-    log_breaks = -(jnp.maximum(logits, 0.0) + soft)
-    log_stops = jnp.minimum(logits, 0.0) - soft
-    sums = jnp.sum(
-        jnp.dot(bf16_parts(log_breaks, row, 3), tri_buf[...], preferred_element_type=jnp.float32),
-        axis=0, keepdims=True,
-    )
-    weights = jnp.exp(log_stops + sums[:, :span])
-    share = jnp.sum(
-        jnp.dot(bf16_parts(weights, row, 2), values, preferred_element_type=jnp.float32),
-        axis=0, keepdims=True,
-    )
     total = sums[:, padded - LANES :]
     lane = lax.broadcasted_iota(jnp.int32, (1, LANES), 1) - (LANES - 3)
     terms = jnp.zeros_like(total)
@@ -134,7 +131,7 @@
 def front(x, new, gain, w_key, w_value, w_query, offset, slots, sub):
     span, width = x.shape
     padded = -(-(span + 3) // LANES) * LANES
-    n_copies = 6 + span // CHUNK
+    n_copies = 4 + span // CHUNK + 2 * (width // SLICE)
     return pl.pallas_call(
         functools.partial(front_kernel, slots=slots, sub=sub),
         out_shape=pltpu.VMEM((slots, 8, LANES), jnp.bfloat16),

time: 47.8 us -> 46.9 us (0.981)
  Pallas kernels: 6.02 us -> 5.14 us
    pallas_call x1, Pallas kernels: 3.84 us -> 2.96 us  [front(): pl.pallas_call(functools.partial(front_kernel, slots=slots, sub=sub), out...]
where the time goes in v3:
time: 46.9 us; the launch traced here: 46.7 us
  blocking collectives  32.6 us (70%)
  starting transfers between devices  6.56 us (14%)
  Pallas kernels  5.14 us (11%)
  waiting for transfers between devices  1.73 us (4%)
  between operations  0.64 us (1%)
    all_to_all x1, blocking collectives, shards(): lax.all_to_all(outgoing, SP, split_axis=0, concat_axis=0, tiled=True, axi...  32.6 us
    all_to_all x1, starting transfers between devices, shards(): lax.all_to_all(own, TP, split_axis=0, concat_axis=0, tiled=True, axis_ind...  6.56 us
    pallas_call x1, Pallas kernels, front(): pl.pallas_call(functools.partial(front_kernel, slots=slots, sub=sub), out...  2.96 us
    all_to_all x1, waiting for transfers between devices, shards(): lax.all_to_all(own, TP, split_axis=0, concat_axis=0, tiled=True, axis_ind...  1.73 us
  transfers between devices with their start and end apart: 1, of which 1 were waited for; matrix products, arithmetic and copies ran while one was open for 0% of the time, Pallas kernels for 2%

profile of v3, /device:TPU:1, one launch (start us, length us, event | category | flops | bytes accessed | tf_op | source)
XLA Modules:
  0.0 46.7 jit_solution(13734173059433985546)
XLA Ops:
  0.6 3.0 %front.1 = bf16[96,8,128]{2,1,0:T(8,128)(2,1)S(1)} custom-call(bf16[288,2048]{1,0:T(8,128)(2,1)} %x_hbm.1, bf16[16,128]{1,0:T(8,128)(2,1)} %bitcast.11, f32[16,128]{1,0:T(8,128)} %bitcast.10, bf16[2048,128]{1,0:T(8,128)(2,1)} %wk_hbm.1, bf16[2048,128]{1,0:T(8,128)(2,1)} %wv_hbm.1, bf16[2048,128]{1,0:T(8,128)(2,1)} %wq_hbm.1, f32[1,288]{1,0:T(1,128)} %bitcast.13), custom_call_target="tpu_custom_call" | custom-call | tf_op jit(solution)/shard_map/front/pallas_call | solution.py:135
  3.6 32.6 %all_to_all.10.arrived_ref = bf16[96,8,128]{2,1,0:T(8,128)(2,1)S(1)} all-to-all(bf16[96,8,128]{2,1,0:T(8,128)(2,1)S(1)} %front.1), channel_id=1, replica_groups={{608,616,624,632,640,648,656,664,672,680,688,696,704,712,720,728,736,74..., dimensions={0} | all-to-all | bytes 393216 | tf_op jit(solution)/shard_map/all_to_all | solution.py:248
  36.2 0.9 %join.1 = bf16[8,1,128]{2,1,0:T(2,128)(2,1)} custom-call(bf16[96,8,128]{2,1,0:T(8,128)(2,1)S(1)} %all_to_all.10.arrived_ref), custom_call_target="tpu_custom_call" | custom-call | tf_op jit(solution)/shard_map/join/pallas_call | solution.py:179
  37.1 6.6 %all-to-all-start.1 = ((bf16[8,1,128]{2,1,0:T(2,128)(2,1)}), bf16[8,1,128]{2,1,0:T(2,128)(2,1)S(1)}, u32[]{:S(2)}, u32[]{:S(2)}) async-start(bf16[8,1,128]{2,1,0:T(2,128)(2,1)} %join.1), calls=%async_computation.1 | async-start | bytes 8192 | tf_op jit(solution)/shard_map/all_to_all | solution.py:254
  43.6 0.7 %unpack.1 = (bf16[3,96,128]{2,1,0:T(8,128)(2,1)}, bf16[3,96,128]{2,1,0:T(8,128)(2,1)}) custom-call(bf16[96,8,128]{2,1,0:T(8,128)(2,1)S(1)} %all_to_all.10.arrived_ref), custom_call_target="tpu_custom_call" | custom-call | tf_op jit(solution)/shard_map/unpack/pallas_call | solution.py:204
  44.3 1.7 %all-to-all-done.1.heads_ref = bf16[8,1,128]{2,1,0:T(2,128)(2,1)S(1)} async-done(((bf16[8,1,128]{2,1,0:T(2,128)(2,1)}), bf16[8,1,128]{2,1,0:T(2,128)(2,1)S(1)}, u32[]{:S(2)}, u32[]{:S(2)}) %all-to-all-start.1) | async-done | bytes 2080 | tf_op jit(solution)/shard_map/all_to_all | solution.py:254
  46.1 0.6 %finish.1 = bf16[8,128]{1,0:T(8,128)(2,1)} custom-call(bf16[8,1,128]{2,1,0:T(2,128)(2,1)S(1)} %all-to-all-done.1.heads_ref), custom_call_target="tpu_custom_call" | custom-call | tf_op jit(solution)/shard_map/finish/pallas_call | solution.py:227
Async XLA Ops:
  37.1 9.0 %all-to-all-start.1 = ((bf16[8,1,128]{2,1,0:T(2,128)(2,1)}), bf16[8,1,128]{2,1,0:T(2,128)(2,1)S(1)}, u32[]{:S(2)}, u32[]{:S(2)}) async-start(bf16[8,1,128]{2,1,0:T(2,128)(2,1)} %join.1), calls=%async_computation.1 | async-start | bytes 8192 | tf_op jit(solution)/shard_map/all_to_all | solution.py:254

commit v4 on v3

--- a/solution.py
+++ b/solution.py
@@ -11,9 +11,8 @@
 LANES = 128
 SP = "sp"
 TP = "tp"
-FIRST_RANK = 76
+FIRST_RANK = 68
 CHUNK = 96
-SLICE = 2048
 TP_FIRST = 5
 
 
@@ -35,14 +34,11 @@
     span, width = x_buf.shape
     padded = tri_buf.shape[1]
     row_blocks = [pl.ds(c * CHUNK, CHUNK) for c in range(span // CHUNK)]
-    slices = [pl.ds(c * SLICE, SLICE) for c in range(width // SLICE)]
     columns = [pl.ds(c * LANES, LANES) for c in range(width // LANES)]
 
     sources = [(gain_hbm, gain_buf), (next_hbm, next_buf), (offset_hbm, offset_buf), (wq_hbm, wq_buf)]
     sources += [(x_hbm.at[rows, :], x_buf.at[rows, :]) for rows in row_blocks]
-    for rows in slices:
-        sources += [(wk_hbm.at[rows, :], w_buf.at[rows, pl.ds(0, HEAD_DIM)])]
-        sources += [(wv_hbm.at[rows, :], w_buf.at[rows, pl.ds(HEAD_DIM, HEAD_DIM)])]
+    sources += [(wk_hbm, w_buf.at[:, pl.ds(0, HEAD_DIM)]), (wv_hbm, w_buf.at[:, pl.ds(HEAD_DIM, HEAD_DIM)])]
     copies = [pltpu.make_async_copy(source, target, sems.at[n]) for n, (source, target) in enumerate(sources)]
     for copy in copies:
         copy.start()
@@ -82,8 +78,8 @@
         jnp.dot(normed_buf[r : r + 144, :], w_buf[...], preferred_element_type=jnp.float32)
         for r in range(0, span, 144)
     ], axis=0)
-    k_buf[...] = both[:, :HEAD_DIM]
-    v_buf[...] = both[:, HEAD_DIM:]
+    k_buf[:span, :] = both[:, :HEAD_DIM]
+    v_buf[:span, :] = both[:, HEAD_DIM:]
     keys = both[:, :HEAD_DIM].astype(jnp.bfloat16)
     values = both[:, HEAD_DIM:].astype(jnp.bfloat16)
     logits = (
@@ -125,13 +121,13 @@
         rest = rest - term
     wide_out[pl.ds(2 * sub, slots, stride=8), :] = jnp.broadcast_to(share, (slots, LANES))
     wide_out[pl.ds(2 * sub + 1, slots, stride=8), :] = jnp.broadcast_to(terms, (slots, LANES))
-    out_ref[...] = wide_out[...].reshape(slots, 8, LANES).astype(jnp.bfloat16)
+    out_ref[...] = wide_out[: slots * 8, :].reshape(slots, 8, LANES).astype(jnp.bfloat16)
 
 
 def front(x, new, gain, w_key, w_value, w_query, offset, slots, sub):
     span, width = x.shape
     padded = -(-(span + 3) // LANES) * LANES
-    n_copies = 4 + span // CHUNK + 2 * (width // SLICE)
+    n_copies = 6 + span // CHUNK
     return pl.pallas_call(
         functools.partial(front_kernel, slots=slots, sub=sub),
         out_shape=pltpu.VMEM((slots, 8, LANES), jnp.bfloat16),
@@ -145,10 +141,10 @@
             pltpu.VMEM((width // LANES, LANES), jnp.float32),
             pltpu.VMEM((1, span), jnp.float32),
             pltpu.VMEM((span, width), jnp.bfloat16),
-            pltpu.VMEM((span, HEAD_DIM), jnp.float32),
-            pltpu.VMEM((span, HEAD_DIM), jnp.float32),
+            pltpu.VMEM((span + 8 * sub, HEAD_DIM), jnp.float32),
+            pltpu.VMEM((span + 8 * sub, HEAD_DIM), jnp.float32),
             pltpu.VMEM((span, padded), jnp.bfloat16),
-            pltpu.VMEM((slots * 8, LANES), jnp.float32),
+            pltpu.VMEM((slots * 8 + 64, LANES), jnp.float32),
             pltpu.SemaphoreType.DMA((n_copies,)),
         ],
         name="front",
@@ -186,9 +182,13 @@
     )(arrived)
 
 
-def unpack_kernel(arrived_ref, key_ref, value_ref, wide, cache, *, sub):
+def finish_kernel(heads_ref, arrived_ref, read_ref, key_ref, value_ref, wide, cache, *, sub):
     slots = arrived_ref.shape[0]
-    wide[...] = arrived_ref[...].astype(jnp.float32).reshape(slots * 8, LANES)
+    heads = read_ref.shape[0]
+    for r in range(heads):
+        h = (r + TP_FIRST) % heads
+        read_ref[h : h + 1, :] = heads_ref[r]
+    wide[: slots * 8, :] = arrived_ref[...].astype(jnp.float32).reshape(slots * 8, LANES)
     for out_ref, base in ((key_ref, 0), (value_ref, sub)):
         for k in range(sub):
             for block, rank, count in (
@@ -196,41 +196,25 @@
                 (0, slots - FIRST_RANK, FIRST_RANK),
             ):
                 cache[pl.ds(block, count), :] = wide[pl.ds(rank * 8 + base + k, count, stride=8), :]
-            out_ref[k] = cache[...].astype(jnp.bfloat16)
-
-
-def unpack(arrived, sub):
+            out_ref[k] = cache[:slots, :].astype(jnp.bfloat16)
+
+
+def finish(heads_read, arrived, sub):
+    heads = heads_read.shape[0]
     slots = arrived.shape[0]
-    caches = pl.pallas_call(
-        functools.partial(unpack_kernel, sub=sub),
-        out_shape=[jax.ShapeDtypeStruct((sub, slots, LANES), jnp.bfloat16)] * 2,
-        in_specs=[pl.BlockSpec(memory_space=pltpu.VMEM)],
-        out_specs=[pl.BlockSpec(memory_space=pltpu.VMEM)] * 2,
+    read, *caches = pl.pallas_call(
+        functools.partial(finish_kernel, sub=sub),
+        out_shape=[jax.ShapeDtypeStruct((heads, LANES), jnp.bfloat16)]
+        + [jax.ShapeDtypeStruct((sub, slots, LANES), jnp.bfloat16)] * 2,
+        in_specs=[pl.BlockSpec(memory_space=pltpu.VMEM)] * 2,
+        out_specs=[pl.BlockSpec(memory_space=pltpu.VMEM)] * 3,
         scratch_shapes=[
-            pltpu.VMEM((slots * 8, LANES), jnp.float32),
-            pltpu.VMEM((slots, LANES), jnp.float32),
+            pltpu.VMEM((slots * 8 + 64, LANES), jnp.float32),
+            pltpu.VMEM((slots + 8, LANES), jnp.float32),
         ],
-        name="unpack",
-    )(arrived)
-    return [cache.transpose(1, 0, 2)[None] for cache in caches]
-
-
-def finish_kernel(heads_ref, out_ref):
-    heads = out_ref.shape[0]
-    for r in range(heads):
-        h = (r + TP_FIRST) % heads
-        out_ref[h : h + 1, :] = heads_ref[r]
-
-
-def finish(heads_read):
-    heads = heads_read.shape[0]
-    return pl.pallas_call(
-        finish_kernel,
-        out_shape=jax.ShapeDtypeStruct((heads, LANES), jnp.bfloat16),
-        in_specs=[pl.BlockSpec(memory_space=pltpu.VMEM)],
-        out_specs=pl.BlockSpec(memory_space=pltpu.VMEM),
         name="finish",
-    )(heads_read).reshape(heads * LANES)
+    )(heads_read, arrived)
+    return *[cache.transpose(1, 0, 2)[None] for cache in caches], read.reshape(heads * LANES)
 
 
 def on_chip(array):
@@ -252,7 +236,7 @@
     own = join( arrived, heads, sub)
     tp_order = [(r + TP_FIRST) % heads for r in range(heads)]
     reading = lax.all_to_all(own, TP, split_axis=0, concat_axis=0, tiled=True, axis_index_groups=[tp_order])
-    return *unpack(arrived, sub), finish(on_chip(reading))
+    return finish(on_chip(reading), arrived, sub)
 
 
 def solution(mesh):

time: 46.9 us -> 45.7 us (0.974)
  blocking collectives: 32.6 us -> 40.8 us
  starting transfers between devices: 6.56 us -> 0 us
  waiting for transfers between devices: 1.73 us -> 0 us
  Pallas kernels: 5.14 us -> 3.96 us
    all_to_all x0 -> x1, blocking collectives: none -> 8.62 us  [shards(): lax.all_to_all(own, TP, split_axis=0, concat_axis=0, tiled=True, axis_ind...]
    all_to_all x1 -> x0, starting transfers between devices: 6.56 us -> none  [shards(): lax.all_to_all(own, TP, split_axis=0, concat_axis=0, tiled=True, axis_ind...]
    all_to_all x1 -> x0, waiting for transfers between devices: 1.73 us -> none  [shards(): lax.all_to_all(own, TP, split_axis=0, concat_axis=0, tiled=True, axis_ind...]
    pallas_call x1, Pallas kernels: 0.85 us -> 0.26 us  [join(): pl.pallas_call(functools.partial(join_kernel, sub=sub), out_shape=pltpu.V...]
    pallas_call x2 -> x1, Pallas kernels: 1.32 us -> 0.74 us  [finish(): pl.pallas_call(functools.partial(finish_kernel, sub=sub), out_shape=[jax....]
  transfers between devices with their start and end apart: 1 -> 0, of which waited for: 1 -> 0; matrix products, arithmetic and copies ran while one was open for 0% -> 0% of each run, Pallas kernels for 2% -> 0%
where the time goes in v4:
time: 45.7 us; the launch traced here: 45.4 us
  blocking collectives  40.8 us (89%)
  Pallas kernels  3.96 us (9%)
  between operations  0.64 us (1%)
    all_to_all x1, blocking collectives, shards(): lax.all_to_all(outgoing, SP, split_axis=0, concat_axis=0, tiled=True, axi...  32.2 us
    all_to_all x1, blocking collectives, shards(): lax.all_to_all(own, TP, split_axis=0, concat_axis=0, tiled=True, axis_ind...  8.62 us
    pallas_call x1, Pallas kernels, front(): pl.pallas_call(functools.partial(front_kernel, slots=slots, sub=sub), out...  2.96 us

profile of v4, /device:TPU:1, one launch (start us, length us, event | category | flops | bytes accessed | tf_op | source)
XLA Modules:
  0.0 45.4 jit_solution(13094354933268156084)
XLA Ops:
  0.6 3.0 %front.1 = bf16[96,8,128]{2,1,0:T(8,128)(2,1)S(1)} custom-call(bf16[288,2048]{1,0:T(8,128)(2,1)} %x_hbm.1, bf16[16,128]{1,0:T(8,128)(2,1)} %bitcast.11, f32[16,128]{1,0:T(8,128)} %bitcast.10, bf16[2048,128]{1,0:T(8,128)(2,1)} %wk_hbm.1, bf16[2048,128]{1,0:T(8,128)(2,1)} %wv_hbm.1, bf16[2048,128]{1,0:T(8,128)(2,1)} %wq_hbm.1, f32[1,288]{1,0:T(1,128)} %bitcast.12), custom_call_target="tpu_custom_call" | custom-call | tf_op jit(solution)/shard_map/front/pallas_call | solution.py:131
  3.6 32.2 %all_to_all.10.arrived_ref = bf16[96,8,128]{2,1,0:T(8,128)(2,1)S(1)} all-to-all(bf16[96,8,128]{2,1,0:T(8,128)(2,1)S(1)} %front.1), channel_id=1, replica_groups={{544,552,560,568,576,584,592,600,608,616,624,632,640,648,656,664,672,68..., dimensions={0} | all-to-all | bytes 393216 | tf_op jit(solution)/shard_map/all_to_all | solution.py:232
  35.8 0.3 join.1
  36.1 8.6 %all_to_all.11.heads_ref = bf16[8,1,128]{2,1,0:T(2,128)(2,1)S(1)} all-to-all(bf16[8,1,128]{2,1,0:T(2,128)(2,1)S(1)} %join.1), channel_id=1, replica_groups={{5,6,7,0,1,2,3,4},{13,14,15,8,9,10,11,12},{21,22,23,16,17,18,19,20},{29..., dimensions={0} | all-to-all | bytes 4096 | tf_op jit(solution)/shard_map/all_to_all | solution.py:238
  44.7 0.7 %finish.1 = (bf16[8,128]{1,0:T(8,128)(2,1)}, bf16[3,96,128]{2,1,0:T(8,128)(2,1)}, bf16[3,96,128]{2,1,0:T(8,128)(2,1)}) custom-call(bf16[8,1,128]{2,1,0:T(2,128)(2,1)S(1)} %all_to_all.11.heads_ref, bf16[96,8,128]{2,1,0:T(8,128)(2,1)S(1)} %all_to_all.10.arrived_ref), custom_call_target="tpu_custom_call" | custom-call | tf_op jit(solution)/shard_map/finish/pallas_call | solution.py:205

commit v5 on v4

--- a/solution.py
+++ b/solution.py
@@ -36,13 +36,14 @@
     row_blocks = [pl.ds(c * CHUNK, CHUNK) for c in range(span // CHUNK)]
     columns = [pl.ds(c * LANES, LANES) for c in range(width // LANES)]
 
-    sources = [(gain_hbm, gain_buf), (next_hbm, next_buf), (offset_hbm, offset_buf), (wq_hbm, wq_buf)]
+    sources = [(gain_hbm, gain_buf), (next_hbm, next_buf), (offset_hbm, offset_buf)]
     sources += [(x_hbm.at[rows, :], x_buf.at[rows, :]) for rows in row_blocks]
     sources += [(wk_hbm, w_buf.at[:, pl.ds(0, HEAD_DIM)]), (wv_hbm, w_buf.at[:, pl.ds(HEAD_DIM, HEAD_DIM)])]
+    sources += [(wq_hbm, wq_buf)]
     copies = [pltpu.make_async_copy(source, target, sems.at[n]) for n, (source, target) in enumerate(sources)]
     for copy in copies:
         copy.start()
-    gain_copy, next_copy, offset_copy, wq_copy, *more = copies
+    gain_copy, next_copy, offset_copy, *more, wq_copy = copies
     x_copies, w_copies = more[: len(row_blocks)], more[len(row_blocks) :]
 
     later = lax.broadcasted_iota(jnp.int32, (span, padded), 0) > lax.broadcasted_iota(jnp.int32, (span, padded), 1)
@@ -58,8 +59,6 @@
         [jnp.broadcast_to(new_normed[k : k + 1, :], (8, LANES)) for k in range(width // LANES)], axis=1
     ).astype(jnp.bfloat16)
     offset_copy.wait()
-    wq_copy.wait()
-    query = jnp.dot(new_row, wq_buf[...], preferred_element_type=jnp.float32).astype(jnp.bfloat16)
 
     for rows, copy in zip(row_blocks, x_copies):
         copy.wait()
@@ -74,10 +73,12 @@
 
     w_copies[0].wait()
     w_copies[1].wait()
-    both = jnp.concatenate([
-        jnp.dot(normed_buf[r : r + 144, :], w_buf[...], preferred_element_type=jnp.float32)
-        for r in range(0, span, 144)
-    ], axis=0)
+    halves = [pl.ds(r, span // 2) for r in (0, span // 2)]
+    upper = jnp.dot(normed_buf[halves[0], :], w_buf[...], preferred_element_type=jnp.float32)
+    lower = jnp.dot(normed_buf[halves[1], :], w_buf[...], preferred_element_type=jnp.float32)
+    wq_copy.wait()
+    query = jnp.dot(new_row, wq_buf[...], preferred_element_type=jnp.float32).astype(jnp.bfloat16)
+    both = jnp.concatenate([upper, lower], axis=0)
     k_buf[:span, :] = both[:, :HEAD_DIM]
     v_buf[:span, :] = both[:, HEAD_DIM:]
     keys = both[:, :HEAD_DIM].astype(jnp.bfloat16)

time: 45.7 us -> 45.6 us (level)
  no operation moved by 1% of the time
where the time goes in v5:
time: 45.6 us; the launch traced here: 45.3 us
  blocking collectives  40.8 us (89%)
  Pallas kernels  3.87 us (8%)
  between operations  0.64 us (1%)
    all_to_all x1, blocking collectives, shards(): lax.all_to_all(outgoing, SP, split_axis=0, concat_axis=0, tiled=True, axi...  32.2 us
    all_to_all x1, blocking collectives, shards(): lax.all_to_all(own, TP, split_axis=0, concat_axis=0, tiled=True, axis_ind...  8.62 us
    pallas_call x1, Pallas kernels, front(): pl.pallas_call(functools.partial(front_kernel, slots=slots, sub=sub), out...  2.87 us

profile of v5, /device:TPU:1, one launch (start us, length us, event | category | flops | bytes accessed | tf_op | source)
XLA Modules:
  0.0 45.3 jit_solution(18119056278745664596)
XLA Ops:
  0.6 2.9 %front.1 = bf16[96,8,128]{2,1,0:T(8,128)(2,1)S(1)} custom-call(bf16[288,2048]{1,0:T(8,128)(2,1)} %x_hbm.1, bf16[16,128]{1,0:T(8,128)(2,1)} %bitcast.11, f32[16,128]{1,0:T(8,128)} %bitcast.10, bf16[2048,128]{1,0:T(8,128)(2,1)} %wk_hbm.1, bf16[2048,128]{1,0:T(8,128)(2,1)} %wv_hbm.1, bf16[2048,128]{1,0:T(8,128)(2,1)} %wq_hbm.1, f32[1,288]{1,0:T(1,128)} %bitcast.12), custom_call_target="tpu_custom_call" | custom-call | tf_op jit(solution)/shard_map/front/pallas_call | solution.py:132
  3.5 32.2 %all_to_all.10.arrived_ref = bf16[96,8,128]{2,1,0:T(8,128)(2,1)S(1)} all-to-all(bf16[96,8,128]{2,1,0:T(8,128)(2,1)S(1)} %front.1), channel_id=1, replica_groups={{544,552,560,568,576,584,592,600,608,616,624,632,640,648,656,664,672,68..., dimensions={0} | all-to-all | bytes 393216 | tf_op jit(solution)/shard_map/all_to_all | solution.py:233
  35.7 0.3 join.1
  36.0 8.6 %all_to_all.11.heads_ref = bf16[8,1,128]{2,1,0:T(2,128)(2,1)S(1)} all-to-all(bf16[8,1,128]{2,1,0:T(2,128)(2,1)S(1)} %join.1), channel_id=1, replica_groups={{5,6,7,0,1,2,3,4},{13,14,15,8,9,10,11,12},{21,22,23,16,17,18,19,20},{29..., dimensions={0} | all-to-all | bytes 4096 | tf_op jit(solution)/shard_map/all_to_all | solution.py:239
  44.6 0.7 %finish.1 = (bf16[8,128]{1,0:T(8,128)(2,1)}, bf16[3,96,128]{2,1,0:T(8,128)(2,1)}, bf16[3,96,128]{2,1,0:T(8,128)(2,1)}) custom-call(bf16[8,1,128]{2,1,0:T(2,128)(2,1)S(1)} %all_to_all.11.heads_ref, bf16[96,8,128]{2,1,0:T(8,128)(2,1)S(1)} %all_to_all.10.arrived_ref), custom_call_target="tpu_custom_call" | custom-call | tf_op jit(solution)/shard_map/finish/pallas_call | solution.py:206

commit v6 on v5

--- a/solution.py
+++ b/solution.py
@@ -155,9 +155,17 @@
     )
 
 
-def join_kernel(arrived_ref, out_ref, wide, *, sub):
+def unpack(wide, packed, sub):
+    slots = packed.shape[1]
+    for c in range(2 * sub):
+        low = wide[pl.ds((slots - FIRST_RANK) * 8 + c, FIRST_RANK, stride=8), :]
+        high = wide[pl.ds(c, slots - FIRST_RANK, stride=8), :]
+        packed[c] = jnp.concatenate([low, high], axis=0).astype(jnp.bfloat16)
+
+
+def join_kernel(arrived_ref, out_ref, packed_ref, wide, *, sub):
     slots = arrived_ref.shape[0]
-    wide[...] = arrived_ref[...].astype(jnp.float32).reshape(slots * 8, LANES)
+    wide[: slots * 8, :] = arrived_ref[...].astype(jnp.float32).reshape(slots * 8, LANES)
     shares = wide[pl.ds(2 * sub, slots, stride=8), :]
     terms = wide[pl.ds(2 * sub + 1, slots, stride=8), :].astype(jnp.bfloat16)
 
@@ -170,51 +178,77 @@
     own = jnp.sum(jnp.exp(carried) * shares, axis=0, keepdims=True)
     out_ref[...] = jnp.broadcast_to(own[None], out_ref.shape).astype(jnp.bfloat16)
 
+    @pl.when(lax.rem(lax.axis_index(TP), 2) == 1)
+    def _():
+        unpack(wide, packed_ref, sub)
+
 
 def join(arrived, heads, sub):
     slots = arrived.shape[0]
     return pl.pallas_call(
         functools.partial(join_kernel, sub=sub),
-        out_shape=pltpu.VMEM((heads, 1, LANES), jnp.bfloat16),
+        out_shape=[
+            pltpu.VMEM((heads, 1, LANES), jnp.bfloat16),
+            pltpu.VMEM((2 * sub, slots, LANES), jnp.bfloat16),
+        ],
         in_specs=[pl.BlockSpec(memory_space=pltpu.VMEM)],
-        out_specs=pl.BlockSpec(memory_space=pltpu.VMEM),
-        scratch_shapes=[pltpu.VMEM((slots * 8, LANES), jnp.float32)],
+        out_specs=[pl.BlockSpec(memory_space=pltpu.VMEM)] * 2,
+        scratch_shapes=[pltpu.VMEM((slots * 8 + 64, LANES), jnp.float32)],
         name="join",
     )(arrived)
 
 
-def finish_kernel(heads_ref, arrived_ref, read_ref, key_ref, value_ref, wide, cache, *, sub):
+def finish_kernel(heads_ref, arrived_ref, packed_ref, read_hbm, key_hbm, value_hbm, read_buf, wide, packed_here, sems, *, sub):
     slots = arrived_ref.shape[0]
-    heads = read_ref.shape[0]
+    heads = read_buf.shape[0]
+    odd = lax.rem(lax.axis_index(TP), 2) == 1
+
+    def caches_from(packed):
+        return [
+            pltpu.make_async_copy(packed.at[pl.ds(c * sub, sub)], target, sems.at[c])
+            for c, target in enumerate((key_hbm, value_hbm))
+        ]
+
+    @pl.when(odd)
+    def _():
+        for copy in caches_from(packed_ref):
+            copy.start()
+
     for r in range(heads):
         h = (r + TP_FIRST) % heads
-        read_ref[h : h + 1, :] = heads_ref[r]
-    wide[: slots * 8, :] = arrived_ref[...].astype(jnp.float32).reshape(slots * 8, LANES)
-    for out_ref, base in ((key_ref, 0), (value_ref, sub)):
-        for k in range(sub):
-            for block, rank, count in (
-                (FIRST_RANK, 0, slots - FIRST_RANK),
-                (0, slots - FIRST_RANK, FIRST_RANK),
-            ):
-                cache[pl.ds(block, count), :] = wide[pl.ds(rank * 8 + base + k, count, stride=8), :]
-            out_ref[k] = cache[:slots, :].astype(jnp.bfloat16)
-
-
-def finish(heads_read, arrived, sub):
+        read_buf[h : h + 1, :] = heads_ref[r]
+    read_copy = pltpu.make_async_copy(read_buf, read_hbm, sems.at[2])
+    read_copy.start()
+
+    @pl.when(jnp.logical_not(odd))
+    def _():
+        wide[: slots * 8, :] = arrived_ref[...].astype(jnp.float32).reshape(slots * 8, LANES)
+        unpack(wide, packed_here, sub)
+        for copy in caches_from(packed_here):
+            copy.start()
+
+    for copy in caches_from(packed_here):
+        copy.wait()
+    read_copy.wait()
+
+
+def finish(heads_read, arrived, packed, sub):
     heads = heads_read.shape[0]
     slots = arrived.shape[0]
     read, *caches = pl.pallas_call(
         functools.partial(finish_kernel, sub=sub),
         out_shape=[jax.ShapeDtypeStruct((heads, LANES), jnp.bfloat16)]
         + [jax.ShapeDtypeStruct((sub, slots, LANES), jnp.bfloat16)] * 2,
-        in_specs=[pl.BlockSpec(memory_space=pltpu.VMEM)] * 2,
-        out_specs=[pl.BlockSpec(memory_space=pltpu.VMEM)] * 3,
+        in_specs=[pl.BlockSpec(memory_space=pltpu.VMEM)] * 3,
+        out_specs=[pl.BlockSpec(memory_space=pl.ANY)] * 3,
         scratch_shapes=[
+            pltpu.VMEM((heads, LANES), jnp.bfloat16),
             pltpu.VMEM((slots * 8 + 64, LANES), jnp.float32),
-            pltpu.VMEM((slots + 8, LANES), jnp.float32),
+            pltpu.VMEM((2 * sub, slots, LANES), jnp.bfloat16),
+            pltpu.SemaphoreType.DMA((3,)),
         ],
         name="finish",
-    )(heads_read, arrived)
+    )(heads_read, arrived, packed)
     return *[cache.transpose(1, 0, 2)[None] for cache in caches], read.reshape(heads * LANES)
 
 
@@ -234,10 +268,10 @@
         outgoing, SP, split_axis=0, concat_axis=0, tiled=True, axis_index_groups=[order]
     )
     arrived = on_chip(arrived)
-    own = join( arrived, heads, sub)
+    own, packed = join(arrived, heads, sub)
     tp_order = [(r + TP_FIRST) % heads for r in range(heads)]
     reading = lax.all_to_all(own, TP, split_axis=0, concat_axis=0, tiled=True, axis_index_groups=[tp_order])
-    return finish(on_chip(reading), arrived, sub)
+    return finish(on_chip(reading), arrived, on_chip(packed), sub)
 
 
 def solution(mesh):

time: 45.6 us -> 45.5 us (level)
  no operation moved by 1% of the time
where the time goes in v6:
time: 45.5 us; the launch traced here: 45.3 us
  blocking collectives  40.8 us (90%)
  Pallas kernels  3.86 us (8%)
  between operations  0.65 us (1%)
    all_to_all x1, blocking collectives, shards(): lax.all_to_all(outgoing, SP, split_axis=0, concat_axis=0, tiled=True, axi...  32.2 us
    all_to_all x1, blocking collectives, shards(): lax.all_to_all(own, TP, split_axis=0, concat_axis=0, tiled=True, axis_ind...  8.59 us
    pallas_call x1, Pallas kernels, front(): pl.pallas_call(functools.partial(front_kernel, slots=slots, sub=sub), out...  2.87 us

profile of v6, /device:TPU:1, one launch (start us, length us, event | category | flops | bytes accessed | tf_op | source)
XLA Modules:
  0.0 45.3 jit_solution(992394511230501198)
XLA Ops:
  0.6 2.9 %front.1 = bf16[96,8,128]{2,1,0:T(8,128)(2,1)S(1)} custom-call(bf16[288,2048]{1,0:T(8,128)(2,1)} %x_hbm.1, bf16[16,128]{1,0:T(8,128)(2,1)} %bitcast.11, f32[16,128]{1,0:T(8,128)} %bitcast.10, bf16[2048,128]{1,0:T(8,128)(2,1)} %wk_hbm.1, bf16[2048,128]{1,0:T(8,128)(2,1)} %wv_hbm.1, bf16[2048,128]{1,0:T(8,128)(2,1)} %wq_hbm.1, f32[1,288]{1,0:T(1,128)} %bitcast.12), custom_call_target="tpu_custom_call" | custom-call | tf_op jit(solution)/shard_map/front/pallas_call | solution.py:132
  3.5 32.2 %all_to_all.10.arrived_ref = bf16[96,8,128]{2,1,0:T(8,128)(2,1)S(1)} all-to-all(bf16[96,8,128]{2,1,0:T(8,128)(2,1)S(1)} %front.1), channel_id=1, replica_groups={{544,552,560,568,576,584,592,600,608,616,624,632,640,648,656,664,672,68..., dimensions={0} | all-to-all | bytes 393216 | tf_op jit(solution)/shard_map/all_to_all | solution.py:267
  35.7 0.3 join.1
  36.0 8.6 %all_to_all.11.heads_ref = bf16[8,1,128]{2,1,0:T(2,128)(2,1)S(1)} all-to-all(bf16[8,1,128]{2,1,0:T(2,128)(2,1)S(1)} %get-tuple-element.8), channel_id=1, replica_groups={{5,6,7,0,1,2,3,4},{13,14,15,8,9,10,11,12},{21,22,23,16,17,18,19,20},{29..., dimensions={0} | all-to-all | bytes 4096 | tf_op jit(solution)/shard_map/all_to_all | solution.py:273
  44.6 0.7 %finish.1 = (bf16[8,128]{1,0:T(8,128)(2,1)}, bf16[3,96,128]{2,1,0:T(8,128)(2,1)}, bf16[3,96,128]{2,1,0:T(8,128)(2,1)}) custom-call(bf16[8,1,128]{2,1,0:T(2,128)(2,1)S(1)} %all_to_all.11.heads_ref, bf16[96,8,128]{2,1,0:T(8,128)(2,1)S(1)} %all_to_all.10.arrived_ref, bf16[6,96,128]{2,1,0:T(8,128)(2,1)S(1)} %get-tuple-element.9.packed_ref), custom_call_target="tpu_custom_call" | custom-call | tf_op jit(solution)/shard_map/finish/pallas_call | solution.py:238

commit v7 on v5

--- a/solution.py
+++ b/solution.py
@@ -81,27 +81,6 @@
     both = jnp.concatenate([upper, lower], axis=0)
     k_buf[:span, :] = both[:, :HEAD_DIM]
     v_buf[:span, :] = both[:, HEAD_DIM:]
-    keys = both[:, :HEAD_DIM].astype(jnp.bfloat16)
-    values = both[:, HEAD_DIM:].astype(jnp.bfloat16)
-    logits = (
-        lax.dot_general(query, keys, (((1,), (1,)), ((), ())), preferred_element_type=jnp.float32)
-        * HEAD_DIM ** (-0.5)
-        + offset_buf[...]
-    )
-    row = lax.broadcasted_iota(jnp.int32, (8, span), 0)
-    soft = jnp.log1p(jnp.exp(-jnp.abs(logits)))
-    log_breaks = -(jnp.maximum(logits, 0.0) + soft)
-    log_stops = jnp.minimum(logits, 0.0) - soft
-    sums = jnp.sum(
-        jnp.dot(bf16_parts(log_breaks, row, 3), tri_buf[...], preferred_element_type=jnp.float32),
-        axis=0, keepdims=True,
-    )
-    weights = jnp.exp(log_stops + sums[:, :span])
-    share = jnp.sum(
-        jnp.dot(bf16_parts(weights, row, 2), values, preferred_element_type=jnp.float32),
-        axis=0, keepdims=True,
-    )
-
     for buf, base in ((k_buf, 0), (v_buf, sub)):
         for k in range(sub):
             for slot, rank, count in (
@@ -111,6 +90,27 @@
                 wide_out[pl.ds(rank * 8 + base + k, count, stride=8), :] = buf[
                     pl.ds(slot * sub + k, count, stride=sub), :
                 ]
+
+    keys = both[:, :HEAD_DIM].astype(jnp.bfloat16)
+    values = both[:, HEAD_DIM:].astype(jnp.bfloat16)
+    logits = (
+        lax.dot_general(query, keys, (((1,), (1,)), ((), ())), preferred_element_type=jnp.float32)
+        * HEAD_DIM ** (-0.5)
+        + offset_buf[...]
+    )
+    row = lax.broadcasted_iota(jnp.int32, (8, span), 0)
+    soft = jnp.log1p(jnp.exp(-jnp.abs(logits)))
+    log_breaks = -(jnp.maximum(logits, 0.0) + soft)
+    log_stops = jnp.minimum(logits, 0.0) - soft
+    sums = jnp.sum(
+        jnp.dot(bf16_parts(log_breaks, row, 3), tri_buf[...], preferred_element_type=jnp.float32),
+        axis=0, keepdims=True,
+    )
+    weights = jnp.exp(log_stops + sums[:, :span])
+    share = jnp.sum(
+        jnp.dot(bf16_parts(weights, row, 2), values, preferred_element_type=jnp.float32),
+        axis=0, keepdims=True,
+    )
 
     total = sums[:, padded - LANES :]
     lane = lax.broadcasted_iota(jnp.int32, (1, LANES), 1) - (LANES - 3)

time: 45.6 us -> 45.6 us (level)
  no operation moved by 1% of the time
where the time goes in v7:
time: 45.6 us; the launch traced here: 45.3 us
  blocking collectives  40.8 us (89%)
  Pallas kernels  3.87 us (8%)
  between operations  0.64 us (1%)
    all_to_all x1, blocking collectives, shards(): lax.all_to_all(outgoing, SP, split_axis=0, concat_axis=0, tiled=True, axi...  32.2 us
    all_to_all x1, blocking collectives, shards(): lax.all_to_all(own, TP, split_axis=0, concat_axis=0, tiled=True, axis_ind...  8.62 us
    pallas_call x1, Pallas kernels, front(): pl.pallas_call(functools.partial(front_kernel, slots=slots, sub=sub), out...  2.87 us

profile of v7, /device:TPU:1, one launch (start us, length us, event | category | flops | bytes accessed | tf_op | source)
XLA Modules:
  0.0 45.3 jit_solution(18119056278745664596)
XLA Ops:
  0.6 2.9 %front.1 = bf16[96,8,128]{2,1,0:T(8,128)(2,1)S(1)} custom-call(bf16[288,2048]{1,0:T(8,128)(2,1)} %x_hbm.1, bf16[16,128]{1,0:T(8,128)(2,1)} %bitcast.11, f32[16,128]{1,0:T(8,128)} %bitcast.10, bf16[2048,128]{1,0:T(8,128)(2,1)} %wk_hbm.1, bf16[2048,128]{1,0:T(8,128)(2,1)} %wv_hbm.1, bf16[2048,128]{1,0:T(8,128)(2,1)} %wq_hbm.1, f32[1,288]{1,0:T(1,128)} %bitcast.12), custom_call_target="tpu_custom_call" | custom-call | tf_op jit(solution)/shard_map/front/pallas_call | solution.py:132
  3.5 32.2 %all_to_all.10.arrived_ref = bf16[96,8,128]{2,1,0:T(8,128)(2,1)S(1)} all-to-all(bf16[96,8,128]{2,1,0:T(8,128)(2,1)S(1)} %front.1), channel_id=1, replica_groups={{544,552,560,568,576,584,592,600,608,616,624,632,640,648,656,664,672,68..., dimensions={0} | all-to-all | bytes 393216 | tf_op jit(solution)/shard_map/all_to_all | solution.py:233
  35.7 0.3 join.1
  36.0 8.6 %all_to_all.11.heads_ref = bf16[8,1,128]{2,1,0:T(2,128)(2,1)S(1)} all-to-all(bf16[8,1,128]{2,1,0:T(2,128)(2,1)S(1)} %join.1), channel_id=1, replica_groups={{5,6,7,0,1,2,3,4},{13,14,15,8,9,10,11,12},{21,22,23,16,17,18,19,20},{29..., dimensions={0} | all-to-all | bytes 4096 | tf_op jit(solution)/shard_map/all_to_all | solution.py:239
  44.6 0.7 %finish.1 = (bf16[8,128]{1,0:T(8,128)(2,1)}, bf16[3,96,128]{2,1,0:T(8,128)(2,1)}, bf16[3,96,128]{2,1,0:T(8,128)(2,1)}) custom-call(bf16[8,1,128]{2,1,0:T(2,128)(2,1)S(1)} %all_to_all.11.heads_ref, bf16[96,8,128]{2,1,0:T(8,128)(2,1)S(1)} %all_to_all.10.arrived_ref), custom_call_target="tpu_custom_call" | custom-call | tf_op jit(solution)/shard_map/finish/pallas_call | solution.py:206
